TPU v7x, 128 devices: a whole 4x4x4 slice. The times are simulated.
128 devices in a mesh: rep: 2 (over x_hi), fs: 16 (over y, x_lo, core), tp: 4 (over z).
Axes of the slice: x: 4 (x_hi: 2, x_lo: 2; x = x_hi * 2 + x_lo), y: 4, z: 4, core: 2. Of those that a mesh axis runs over, the one named last changes fastest.
Arguments:
- tokens: bfloat16 [16384, 2048], P(('rep', 'fs', 'tp')), may hold values from -3 to 3
- mixer_output: bfloat16 [16384, 2048], P(('rep', 'fs', 'tp')), may hold values from -6 to 6
- early_norm: float32 [2048], replicated, may hold values from 0.75 to 1.25
- early_gate: bfloat16 [2048, 5120], P('fs', 'tp'), may hold values from -0.125 to 0.125
- early_value: bfloat16 [2048, 5120], P('fs', 'tp'), may hold values from -0.125 to 0.125
- early_down: bfloat16 [5120, 2048], P('tp', 'fs'), may hold values from -0.078125 to 0.078125
- early_post: float32 [2048], replicated, may hold values from 0.75 to 1.25
- mixer_gain: float32 [2048], replicated, may hold values from 0.75 to 1.25
- later_norm: float32 [2048], replicated, may hold values from 0.75 to 1.25
- later_gate: bfloat16 [2048, 5120], P('fs', 'tp'), may hold values from -0.125 to 0.125
- later_value: bfloat16 [2048, 5120], P('fs', 'tp'), may hold values from -0.125 to 0.125
- later_down: bfloat16 [5120, 2048], P('tp', 'fs'), may hold values from -0.078125 to 0.078125
- later_post: float32 [2048], replicated, may hold values from 0.75 to 1.25
Outputs:
- layer_out: bfloat16 [16384, 2048], P(('rep', 'fs', 'tp'))
All inputs are finite; a program needn't handle non-finite values.
Results may differ from a plain program's by a relative error of at most 0.015.
Values may be sent and summed in bfloat16 or wider, within the bound.
A program may use at most 128 MiB of HBM per device.

v0:
```python
import jax
import jax.numpy as jnp
from jax import lax
from jax.sharding import PartitionSpec as P

epsilon = 1e-06


def over_all(piece, axis, dim, step, start):
    def gathered(part):
        return lax.all_gather(part, axis, axis=dim, tiled=True)

    return step(start, jax.tree.map(gathered, piece), jnp.int32(0))


def own_rows(product, extent, axis):
    everything = product(jnp.int32(0), lax.axis_size(axis) * extent)
    own = lax.psum_scatter(everything.astype(jnp.bfloat16), axis, scatter_dimension=0, tiled=True)
    return own.astype(jnp.float32)


def rms_scale(values, gain):
    values = values.astype(jnp.float32)
    scale = lax.rsqrt(jnp.mean(values * values, axis=-1, keepdims=True) + epsilon)
    return values * scale * gain


def half_branch(normed, gate_piece, value_piece, down_piece):
    all_rows = lax.all_gather(normed, "tp", axis=0, tiled=True)
    empty = jnp.zeros((all_rows.shape[0], gate_piece.shape[1]), jnp.float32)

    def add_rows(totals, pieces, start):
        columns = lax.dynamic_slice_in_dim(all_rows, start, pieces[0].shape[0], 1)
        gate_part = jnp.dot(columns, pieces[0], preferred_element_type=jnp.float32)
        value_part = jnp.dot(columns, pieces[1], preferred_element_type=jnp.float32)
        return (totals[0] + gate_part, totals[1] + value_part)

    gate_sum, value_sum = over_all((gate_piece, value_piece), "fs", 0, add_rows, (empty, empty))
    down_block = lax.all_gather(down_piece, "fs", axis=1, tiled=True)
    hidden = (jax.nn.silu(gate_sum) * value_sum).astype(jnp.bfloat16)

    def row_term(start, count):
        rows = lax.dynamic_slice_in_dim(hidden, start, count, 0)
        return jnp.dot(rows, down_block, preferred_element_type=jnp.float32)

    return own_rows(row_term, normed.shape[0], "tp")


def on_device(
    tokens,
    mixer_output,
    early_norm,
    early_gate,
    early_value,
    early_down,
    early_post,
    mixer_gain,
    later_norm,
    later_gate,
    later_value,
    later_down,
    later_post,
):
    early_in = rms_scale(tokens, early_norm).astype(jnp.bfloat16)
    early_branch = half_branch(early_in, early_gate, early_value, early_down)
    mixed = (
        tokens.astype(jnp.float32)
        + 0.5 * rms_scale(early_branch, early_post)
        + rms_scale(mixer_output, mixer_gain)
    )
    mixed = mixed.astype(jnp.bfloat16)
    later_in = rms_scale(mixed, later_norm).astype(jnp.bfloat16)
    later_branch = half_branch(later_in, later_gate, later_value, later_down)
    layer_out = mixed.astype(jnp.float32) + 0.5 * rms_scale(later_branch, later_post)
    return layer_out.astype(jnp.bfloat16)


def solution(mesh):
    placed = (
        P(("rep", "fs", "tp"), None),
        P(("rep", "fs", "tp"), None),
        P(),
        P("fs", "tp"),
        P("fs", "tp"),
        P("tp", "fs"),
        P(),
        P(),
        P(),
        P("fs", "tp"),
        P("fs", "tp"),
        P("tp", "fs"),
        P(),
    )
    return jax.shard_map(
        on_device,
        mesh=mesh,
        in_specs=placed,
        out_specs=P(("rep", "fs", "tp"), None),
        check_vma=False,
    )
```

profile of v0, /device:TPU:1, one launch (start us, length us, event | category | flops | bytes accessed | tf_op | source)
XLA Modules:
  0.0 436.3 jit_solution(11551723246681318497)
XLA Ops:
  6.5 1.2 fusion.12
  7.8 2.0 fusion.14
  9.9 0.7 all-gather.11.cloned.1.call-update
  10.6 0.7 all-gather.13.cloned.1.call-update
  11.9 31.9 %all-gather.9.cloned.1.call-done = bf16[512,2048]{1,0:T(8,128)(2,1)} async-done(((bf16[128,2048]{1,0:T(8,128)(2,1)}), bf16[512,2048]{1,0:T(8,128)(2,1)}) %all-gather.9.cloned.1.call-update) | async-done | bytes 2097168 | tf_op jit(solution)/shard_map/all_gather | solution.py:29
  43.8 41.4 %all-gather.11.cloned.1.call-done = bf16[2048,1280]{1,0:T(8,128)(2,1)} async-done(((bf16[128,1280]{1,0:T(8,128)(2,1)}), bf16[2048,1280]{1,0:T(8,128)(2,1)}) %all-gather.11.cloned.1.call-update) | async-done | bytes 5242896 | tf_op jit(solution)/shard_map/all_gather | solution.py:11
  85.2 7.5 %fusion.22 = f32[512,1280]{1,0:T(8,128)} fusion(bf16[512,2048]{1,0:T(8,128)(2,1)} %all-gather.9.cloned.1.call-done, bf16[2048,1280]{1,0:T(8,128)(2,1)} %all-gather.11.cloned.1.call-done), kind=kOutput, calls=%fused_computation.42 | convolution fusion | flops 2684354560 | bytes 9961472 | tf_op jit(solution)/shard_map/dot_general | solution.py:34
  92.7 33.5 %all-gather.13.cloned.1.call-done = bf16[2048,1280]{1,0:T(8,128)(2,1)} async-done(((bf16[128,1280]{1,0:T(8,128)(2,1)}), bf16[2048,1280]{1,0:T(8,128)(2,1)}) %all-gather.13.cloned.1.call-update) | async-done | bytes 5242896 | tf_op jit(solution)/shard_map/all_gather | solution.py:11
  126.2 51.3 %all-gather.15.cloned.1.call-done = bf16[1280,2048]{1,0:T(8,128)(2,1)} async-done(((bf16[1280,128]{1,0:T(8,128)(2,1)}), bf16[1280,2048]{1,0:T(8,128)(2,1)}) %all-gather.15.cloned.1.call-update) | async-done | bytes 5242896 | tf_op jit(solution)/shard_map/all_gather | solution.py:39
  177.5 12.5 %convolution_convert_fusion.1 = bf16[512,2048]{1,0:T(8,128)(2,1)} fusion(bf16[1280,2048]{1,0:T(8,128)(2,1)} %all-gather.15.cloned.1.call-done, bf16[512,2048]{1,0:T(8,128)(2,1)S(1)} %copy-done.6, bf16[2048,1280]{1,0:T(8,128)(2,1)} %all-gather.13.cloned.1.call-done, f32[512,1280]{1,0:T(8,128)} %fusion.22), kind=kOutput, calls=%fused_computation.5 | convolution fusion | flops 5373689856 | bytes 17301504 | tf_op jit(solution)/shard_map/dot_general | solution.py:44
  191.2 27.6 %reduce-scatter.3.cloned.1.call-done = bf16[128,2048]{1,0:T(8,128)(2,1)} async-done(((bf16[512,2048]{1,0:T(8,128)(2,1)}), bf16[128,2048]{1,0:T(8,128)(2,1)}) %reduce-scatter.3.cloned.1.call-update) | async-done | bytes 524304 | tf_op jit(solution)/shard_map/reduce_scatter | solution.py:18
  218.9 1.2 fusion.2
  220.1 1.6 fusion.15
  221.8 1.0 fusion.17
  222.8 0.7 all-gather.21.cloned.1.call-update
  224.5 35.3 %all-gather.19.cloned.1.call-done = bf16[2048,1280]{1,0:T(8,128)(2,1)} async-done(((bf16[128,1280]{1,0:T(8,128)(2,1)}), bf16[2048,1280]{1,0:T(8,128)(2,1)}) %all-gather.19.cloned.1.call-update) | async-done | bytes 5242896 | tf_op jit(solution)/shard_map/all_gather | solution.py:11
  259.8 32.1 %all-gather.17.cloned.1.call-done = bf16[512,2048]{1,0:T(8,128)(2,1)} async-done(((bf16[128,2048]{1,0:T(8,128)(2,1)}), bf16[512,2048]{1,0:T(8,128)(2,1)}) %all-gather.17.cloned.1.call-update) | async-done | bytes 2097168 | tf_op jit(solution)/shard_map/all_gather | solution.py:29
  291.9 7.6 %fusion.23 = f32[512,1280]{1,0:T(8,128)} fusion(bf16[512,2048]{1,0:T(8,128)(2,1)} %all-gather.17.cloned.1.call-done, bf16[2048,1280]{1,0:T(8,128)(2,1)} %all-gather.19.cloned.1.call-done), kind=kOutput, calls=%fused_computation.43 | convolution fusion | flops 2684354560 | bytes 9961472 | tf_op jit(solution)/shard_map/dot_general | solution.py:34
  299.5 33.7 %all-gather.21.cloned.1.call-done = bf16[2048,1280]{1,0:T(8,128)(2,1)} async-done(((bf16[128,1280]{1,0:T(8,128)(2,1)}), bf16[2048,1280]{1,0:T(8,128)(2,1)}) %all-gather.21.cloned.1.call-update) | async-done | bytes 5242896 | tf_op jit(solution)/shard_map/all_gather | solution.py:11
  333.3 51.5 %all-gather.23.cloned.1.call-done = bf16[1280,2048]{1,0:T(8,128)(2,1)} async-done(((bf16[1280,128]{1,0:T(8,128)(2,1)}), bf16[1280,2048]{1,0:T(8,128)(2,1)}) %all-gather.23.cloned.1.call-update) | async-done | bytes 5242896 | tf_op jit(solution)/shard_map/all_gather | solution.py:39
  384.7 12.5 %convolution_convert_fusion = bf16[512,2048]{1,0:T(8,128)(2,1)} fusion(bf16[1280,2048]{1,0:T(8,128)(2,1)} %all-gather.23.cloned.1.call-done, bf16[512,2048]{1,0:T(8,128)(2,1)S(1)} %copy-done.7, bf16[2048,1280]{1,0:T(8,128)(2,1)} %all-gather.21.cloned.1.call-done, f32[512,1280]{1,0:T(8,128)} %fusion.23), kind=kOutput, calls=%fused_computation.4 | convolution fusion | flops 5373689856 | bytes 17301504 | tf_op jit(solution)/shard_map/dot_general | solution.py:44
  397.2 28.8 %reduce-scatter.5.cloned.1.call-done = bf16[128,2048]{1,0:T(8,128)(2,1)} async-done(((bf16[512,2048]{1,0:T(8,128)(2,1)}), bf16[128,2048]{1,0:T(8,128)(2,1)}) %reduce-scatter.5.cloned.1.call-update) | async-done | bytes 524304 | tf_op jit(solution)/shard_map/reduce_scatter | solution.py:18
  426.1 1.2 fusion.9
  427.3 2.1 fusion.18
  (39 shorter events, 3.0 us)
Async XLA Ops:
  6.5 37.3 %all-gather.9.cloned.1.call-start = ((), (), s32[]{:S(2)}) async-start(), calls=%async_computation.2 | async-start | bytes 2621440 | tf_op jit(solution)/shard_map/all_gather | solution.py:29
  9.8 75.4 %all-gather.11.cloned.1.call-start = ((), (), s32[]{:S(2)}) async-start(), calls=%async_computation.3 | async-start | bytes 5570560 | tf_op jit(solution)/shard_map/all_gather | solution.py:11
  10.6 115.6 %all-gather.13.cloned.1.call-start = ((), (), s32[]{:S(2)}) async-start(), calls=%async_computation.4 | async-start | bytes 5570560 | tf_op jit(solution)/shard_map/all_gather | solution.py:11
  11.3 166.2 %all-gather.15.cloned.1.call-start = ((), (), s32[]{:S(2)}) async-start(), calls=%async_computation.5 | async-start | bytes 5570560 | tf_op jit(solution)/shard_map/all_gather | solution.py:39
  11.9 207.0 %reduce-scatter.3.cloned.1.call-start = ((), (), s32[]{:S(2)}) async-start(), calls=%async_computation.6 | async-start | bytes 2621440 | tf_op jit(solution)/shard_map/reduce_scatter | solution.py:18
  43.8 133.7 %copy-start.6 = (bf16[512,2048]{1,0:T(8,128)(2,1)S(1)}, bf16[512,2048]{1,0:T(8,128)(2,1)}, u32[]{:S(2)}) copy-start(bf16[512,2048]{1,0:T(8,128)(2,1)} %all-gather.9.cloned.1.call-done) | copy-start | bytes 6291460
  190.0 1.0 copy-start.1
  190.0 30.1 %copy-start = (bf16[128,2048]{1,0:T(8,128)(2,1)S(1)}, bf16[128,2048]{1,0:T(8,128)(2,1)}, u32[]{:S(2)}) copy-start(bf16[128,2048]{1,0:T(8,128)(2,1)} %param.13) | copy-start | bytes 1572868
  190.0 30.1 %copy-start.2 = (f32[2048]{0:T(1024)S(1)}, f32[2048]{0:T(1024)}, u32[]{:S(2)}) copy-start(f32[2048]{0:T(1024)} %param.20) | copy-start | bytes 24580
  190.0 30.1 %copy-start.3 = (f32[2048]{0:T(1024)S(1)}, f32[2048]{0:T(1024)}, u32[]{:S(2)}) copy-start(f32[2048]{0:T(1024)} %param.19) | copy-start | bytes 24580
  190.0 31.8 %copy-start.4 = (f32[2048]{0:T(1024)S(1)}, f32[2048]{0:T(1024)}, u32[]{:S(2)}) copy-start(f32[2048]{0:T(1024)} %param.21) | copy-start | bytes 24580
  190.0 69.8 %all-gather.19.cloned.1.call-start = ((), (), s32[]{:S(2)}) async-start(), calls=%async_computation.8 | async-start | bytes 5570560 | tf_op jit(solution)/shard_map/all_gather | solution.py:11
  190.6 101.3 %all-gather.17.cloned.1.call-start = ((), (), s32[]{:S(2)}) async-start(), calls=%async_computation.7 | async-start | bytes 2621440 | tf_op jit(solution)/shard_map/all_gather | solution.py:29
  222.8 110.5 %all-gather.21.cloned.1.call-start = ((), (), s32[]{:S(2)}) async-start(), calls=%async_computation.9 | async-start | bytes 5570560 | tf_op jit(solution)/shard_map/all_gather | solution.py:11
  223.6 161.2 %all-gather.23.cloned.1.call-start = ((), (), s32[]{:S(2)}) async-start(), calls=%async_computation.10 | async-start | bytes 5570560 | tf_op jit(solution)/shard_map/all_gather | solution.py:39
  224.3 201.8 %reduce-scatter.5.cloned.1.call-start = ((), (), s32[]{:S(2)}) async-start(), calls=%async_computation.11 | async-start | bytes 2621440 | tf_op jit(solution)/shard_map/reduce_scatter | solution.py:18
  291.9 92.8 %copy-start.7 = (bf16[512,2048]{1,0:T(8,128)(2,1)S(1)}, bf16[512,2048]{1,0:T(8,128)(2,1)}, u32[]{:S(2)}) copy-start(bf16[512,2048]{1,0:T(8,128)(2,1)} %all-gather.17.cloned.1.call-done) | copy-start | bytes 6291460
  397.2 30.1 %copy-start.5 = (f32[2048]{0:T(1024)S(1)}, f32[2048]{0:T(1024)}, u32[]{:S(2)}) copy-start(f32[2048]{0:T(1024)} %param.25) | copy-start | bytes 24580
Sparse Core Ops, SparseCore 0:
  9.9 33.8 all-gather.8
  45.5 39.6 all-gather.10
  86.9 39.2 all-gather.12
  127.7 49.7 all-gather.14
  190.2 28.6 reduce-scatter.2
  220.4 39.3 all-gather.18
  261.5 30.3 all-gather.16
  293.6 39.6 all-gather.20
  334.9 49.7 all-gather.22
  397.4 28.6 reduce-scatter.4
where the time goes:
time: 437 us; the launch traced here: 436 us
  waiting for transfers between devices  371 us (85%)
  matrix products  40.1 us (9%)
  between operations  13.6 us (3%)
  other arithmetic  10.7 us (2%)
    all_gather x4, waiting for transfers between devices, gathered(): return lax.all_gather(part, axis, axis=dim, tiled=True)  144 us
    all_gather x2, waiting for transfers between devices, half_branch(): down_block = lax.all_gather(down_piece, 'fs', axis=1, tiled=True)  103 us
    all_gather x2, waiting for transfers between devices, half_branch(): all_rows = lax.all_gather(normed, 'tp', axis=0, tiled=True)  64 us
    reduce_scatter x2, waiting for transfers between devices, own_rows(): lax.psum_scatter(everything.astype(jnp.bfloat16), axis, scatter_dimension...  56.5 us
    dot_general x2, matrix products, row_term(): return jnp.dot(rows, down_block, preferred_element_type=jnp.float32)  25 us
    dot_general x2, matrix products, add_rows(): gate_part = jnp.dot(columns, pieces[0], preferred_element_type=jnp.float32)  15.1 us
  transfers between devices with their start and end apart: 10, of which 10 were waited for; matrix products, arithmetic and copies ran while one was open for 4% of the time, Pallas kernels for 0%

commit v1 on v0

v1 whole, which is shorter than its diff:
```python
import functools

import jax
import jax.numpy as jnp
from jax import lax
from jax.experimental import pallas as pl
from jax.experimental.pallas import tpu as pltpu
from jax.sharding import PartitionSpec as P

MESH = pl.DeviceIdType.MESH
EPS = 1e-06
BF = jnp.bfloat16
F32 = jnp.float32


def kernel(
    tok, mix, en, eg, ev, ed, ep, mg, ln, lg, lv, ld, lp,
    out,
    gbuf, vbuf, dbuf, xbuf, acc, hbuf, tokv, mixv, mixed, gains,
    rs1, rr1, rs2, rr2, keep, br, pbuf,
    loc_sem, w_send, w_recv, p_send, p_recv, ag_send, ag_recv, rs_send, rs_recv,
):
    rep = lax.axis_index("rep")
    fs = lax.axis_index("fs")
    z = lax.axis_index("tp")
    c = lax.rem(fs, 2)
    xl = lax.rem(fs // 2, 2)
    y = fs // 4
    x = rep * 2 + xl

    def mod4(v):
        return lax.rem(v + 8, 4)

    def dev(dx=0, dy=0, dz=0, dc=0):
        nx = mod4(x + dx)
        ny = mod4(y + dy)
        nc = c if dc == 0 else 1 - c
        return (nx // 2, (ny * 2 + lax.rem(nx, 2)) * 2 + nc, mod4(z + dz))

    y_dev = {1: dev(dy=1), -1: dev(dy=-1)}
    x_dev = {1: dev(dx=1), -1: dev(dx=-1)}
    z_dev = {1: dev(dz=1), -1: dev(dz=-1)}
    partner = dev(dc=1)
    everyone = [y_dev[1], y_dev[-1], x_dev[1], x_dev[-1], z_dev[1], z_dev[-1], partner]
    zp, zm, zo = mod4(z + 1), mod4(z - 1), mod4(z + 2)

    def blk_of(dy, dp):
        return mod4(y + dy) * 2 + (xl if dp == 0 else 1 - xl)

    blocks = {(dy, dp): blk_of(dy, dp) for dy in (0, 1, -1, 2) for dp in (0, 1)}

    def unit(r, content, core):
        dy, dp, st, s = content
        blk = blocks[(dy, dp)]
        layer = r // 2
        if r % 2 == 0:
            buf = gbuf if st == 0 else vbuf
            row = pl.multiple_of(blk * 256 + core * 128 + s * 64, 64)
            return buf.at[layer, pl.ds(row, 64), :]
        return dbuf.at[layer, blk, core, pl.ds(st * 640 + s * 320, 320), :]

    def unit_id(content):
        dy, dp, st, s = content
        return (((dy % 4) * 2 + dp) * 2 + st) * 2 + s

    sent = []

    def send(src, dst, send_sem, recv_sem, target):
        copy = pltpu.make_async_remote_copy(src, dst, send_sem, recv_sem, device_id=target, device_id_type=MESH)
        copy.start()
        sent.append(copy)

    def await_copy(dst, send_sem, recv_sem, source):
        pltpu.make_async_remote_copy(dst, dst, send_sem, recv_sem, device_id=source, device_id_type=MESH).wait_recv()

    def tee(sign):
        return 0 if sign > 0 else 1

    def y_recv_content(sign, k):
        t = tee(sign)
        return [(-sign, 0, t, 0), (-sign, 0, t, 1), (2, 0, t, 0), (2, 0, t, 1),
                (-sign, 0, 1 - t, 0), (-sign, 0, 1 - t, 1), (-sign, 1, t, 1)][k]

    def y_send_content(sign, k):
        t = tee(sign)
        return [(0, 0, t, 0), (0, 0, t, 1), (-sign, 0, t, 0), (-sign, 0, t, 1),
                (0, 0, 1 - t, 0), (0, 0, 1 - t, 1), (0, 1, t, 1)][k]

    def x_content(sign, k, dp):
        t = tee(sign)
        return [(0, dp, t, 0), (0, dp, t, 1), (-sign, dp, t, 0), (2, dp, t, 0), (2, dp, t, 1),
                (sign, dp, t, 0), (sign, dp, t, 1)][k]

    have = set()
    partner_have = set()

    def send_y(r, sign, k):
        content = y_send_content(sign, k)
        assert (r, content) in have
        ref = unit(r, content, c)
        send(ref, ref, w_send.at[r, tee(sign), k], w_recv.at[r, tee(sign), k], y_dev[sign])

    def send_x(r, sign, k):
        content = x_content(sign, k, 0)
        assert (r, content) in have
        ref = unit(r, content, c)
        send(ref, ref, w_send.at[r, 2 + tee(sign), k], w_recv.at[r, 2 + tee(sign), k], x_dev[sign])

    def send_partner(r, content):
        ref = unit(r, content, c)
        i = unit_id(content)
        send(ref, ref, p_send.at[r, i], p_recv.at[r, i], partner)

    def need(r, content):
        assert (r, content) in have, (r, content)
        if (r, content) not in partner_have:
            partner_have.add((r, content))
            i = unit_id(content)
            await_copy(unit(r, content, 1 - c), p_send.at[r, i], p_recv.at[r, i], partner)

    def own_y(r):
        wait_local(r)
        for sign in (1, -1):
            send_y(r, sign, 0)
            send_y(r, sign, 1)

    def own_x(r):
        for sign in (1, -1):
            send_x(r, sign, 0)
            send_x(r, sign, 1)

    def own_partner(r):
        for st in (0, 1):
            for s in (0, 1):
                send_partner(r, (0, 0, st, s))

    def y_event(r, j):
        for sign in (1, -1):
            content = y_recv_content(sign, j)
            await_copy(unit(r, content, c), w_send.at[r, tee(sign), j], w_recv.at[r, tee(sign), j], y_dev[-sign])
            have.add((r, content))
            if j == 0:
                send_x(r, sign, 2)
                send_y(r, sign, 2)
            elif j == 1:
                send_y(r, sign, 3)
                send_y(r, sign, 4)
                send_y(r, sign, 5)
            elif j == 2:
                send_x(r, sign, 3)
            elif j == 3:
                send_x(r, sign, 4)
            elif j == 4:
                send_x(r, -sign, 5)
            elif j == 5:
                send_x(r, -sign, 6)
        if r < 3 and j == 3:
            own_y(r + 1)
        if r < 3 and j == 5:
            own_x(r + 1)
        for sign in (1, -1):
            send_partner(r, y_recv_content(sign, j))
        if r < 3 and j == 3:
            own_partner(r + 1)

    def x_event(r, j):
        for sign in (1, -1):
            content = x_content(sign, j, 1)
            lane = 2 + tee(sign)
            await_copy(unit(r, content, c), w_send.at[r, lane, j], w_recv.at[r, lane, j], x_dev[-sign])
            have.add((r, content))
            if j == 1:
                send_y(r, sign, 6)
            send_partner(r, content)

    own = pl.multiple_of(blocks[(0, 0)] * 256 + c * 128, 128)
    weights = {
        0: [(eg, gbuf.at[0, pl.ds(own, 128), :]), (ev, vbuf.at[0, pl.ds(own, 128), :])],
        1: [(ed, dbuf.at[0, blocks[(0, 0)], c])],
        2: [(lg, gbuf.at[1, pl.ds(own, 128), :]), (lv, vbuf.at[1, pl.ds(own, 128), :])],
        3: [(ld, dbuf.at[1, blocks[(0, 0)], c])],
    }
    local = {}
    count = 0
    small = [(tok, tokv)] + [(g, gains.at[i]) for i, g in enumerate((en, ep, mg, ln, lp))] + [(mix, mixv)]
    for name, pairs in [(0, weights[0]), ("small", small), (1, weights[1]), (2, weights[2]), (3, weights[3])]:
        local[name] = []
        for src, dst in pairs:
            copy = pltpu.make_async_copy(src, dst, loc_sem.at[count])
            copy.start()
            local[name].append(copy)
            count += 1

    def wait_local(name):
        for copy in local[name]:
            copy.wait()
        if name != "small":
            for st in (0, 1):
                for s in (0, 1):
                    have.add((name, (0, 0, st, s)))

    barrier = pltpu.get_barrier_semaphore()
    for other in everyone:
        pl.semaphore_signal(barrier, inc=1, device_id=other, device_id_type=MESH)
    pl.semaphore_wait(barrier, len(everyone))

    def x_rows(layer, h, zz, u, n=16):
        row = pl.multiple_of(h * 256 + zz * 64 + u * 16, 16)
        return xbuf.at[layer, pl.ds(row, n), :]

    def ag_send_own(layer, h):
        for u in range(4):
            for sign in (1, -1):
                v = u if sign > 0 else (u + 2) % 4
                ref = x_rows(layer, h, z, v)
                send(ref, ref, ag_send.at[layer, h, tee(sign), v], ag_recv.at[layer, h, tee(sign), v], z_dev[sign])

    def ag_wait_own(layer, h, sign, u):
        zz = zm if sign > 0 else zp
        await_copy(x_rows(layer, h, zz, u), ag_send.at[layer, h, tee(sign), u], ag_recv.at[layer, h, tee(sign), u], z_dev[-sign])

    def ag_forward(layer, h, u):
        for sign in (1, -1):
            v = u if sign > 0 else u + 2
            ag_wait_own(layer, h, sign, v)
            zz = zm if sign > 0 else zp
            ref = x_rows(layer, h, zz, v)
            i = 4 + u
            send(ref, ref, ag_send.at[layer, h, tee(sign), i], ag_recv.at[layer, h, tee(sign), i], z_dev[sign])

    def ag_finish(layer, h):
        for sign in (1, -1):
            for u in (0, 1):
                v = u + 2 if sign > 0 else u
                ag_wait_own(layer, h, sign, v)
        for sign in (1, -1):
            for u in (0, 1):
                v = u if sign > 0 else u + 2
                i = 4 + u
                await_copy(x_rows(layer, h, zo, v), ag_send.at[layer, h, tee(sign), i], ag_recv.at[layer, h, tee(sign), i], z_dev[-sign])

    def rms(v, gain):
        return v * lax.rsqrt(jnp.mean(v * v, axis=-1, keepdims=True) + EPS) * gain

    def early_norm(h):
        def body(i, carry):
            rows = pl.ds(pl.multiple_of(h * 64 + i * 16, 16), 16)
            v = rms(tokv[rows, :].astype(F32), gains[0])
            x_rows(0, h, z, i)[...] = v.astype(BF)
            return carry

        lax.fori_loop(0, 4, body, 0)

    started = set()

    def gemm(st, dy, dp):
        for s in (0, 1):
            need(0, (dy, dp, st, s))
        first = st not in started
        started.add(st)
        base = pl.multiple_of(blocks[(dy, dp)] * 256, 256)
        w = gbuf if st == 0 else vbuf

        def body(n, carry):
            cols = pl.ds(pl.multiple_of(n * 256, 256), 256)
            part = jnp.dot(xbuf[0, :, pl.ds(base, 256)], w[0, pl.ds(base, 256), cols], preferred_element_type=F32)
            if first:
                acc[st, :, cols] = part
            else:
                acc[st, :, cols] += part
            return carry

        lax.fori_loop(0, 5, body, 0)

    def silu_mul(g, v):
        return (g * (1.0 / (1.0 + jnp.exp(-g))) * v).astype(BF)

    def hidden_early(h):
        def body(i, carry):
            rows = pl.ds(pl.multiple_of(h * 256 + i * 16, 16), 16)
            hbuf[rows, :] = silu_mul(acc[0, rows, :], acc[1, rows, :])
            return carry

        lax.fori_loop(0, 16, body, 0)

    def hidden_later(h, n):
        if (h, n) == (0, 0):
            for dy in (0, 1, -1, 2):
                for dp in (0, 1):
                    for st in (0, 1):
                        for s in (0, 1):
                            need(2, (dy, dp, st, s))
        rows = slice(h * 256, h * 256 + 256)
        cols = slice(n * 256, n * 256 + 256)
        xs = xbuf[1, rows, :]
        g = jnp.dot(xs, gbuf[1, :, cols], preferred_element_type=F32)
        v = jnp.dot(xs, vbuf[1, :, cols], preferred_element_type=F32)
        hbuf[rows, cols] = silu_mul(g, v)

    order = (0, 2, -1, 1)

    def rs_refs(kind, layer, h, j, lane):
        return kind.at[layer, h, j, lane]

    def down(layer, h, dy):
        r = 2 * layer + 1
        for dp in (0, 1):
            for st in (0, 1):
                for s in (0, 1):
                    need(r, (dy, dp, st, s))
        j = order.index(dy)
        yy = mod4(y + dy)

        def body(e, carry):
            w = jnp.concatenate([dbuf[layer, yy * 2 + e, 0], dbuf[layer, yy * 2 + e, 1]], axis=1)
            pbuf[:, pl.ds(pl.multiple_of(e * 256, 256), 256)] = jnp.dot(
                hbuf[h * 256 : h * 256 + 256, :], w, preferred_element_type=F32
            )
            return carry

        lax.fori_loop(0, 2, body, 0)

        def rows(zz, half):
            return pl.ds(pl.multiple_of(zz * 64 + half * 32, 32), 32)

        rs1[layer, h, j, 0, 0:32, :] = pbuf[rows(zo, 0), :].astype(BF)
        rs1[layer, h, j, 0, 32:64, :] = pbuf[rows(zp, 1), :].astype(BF)
        rs1[layer, h, j, 1, 0:32, :] = pbuf[rows(zm, 0), :].astype(BF)
        rs1[layer, h, j, 1, 32:64, :] = pbuf[rows(zo, 1), :].astype(BF)
        keep[h, j, 0] = pbuf[rows(zp, 0), :]
        keep[h, j, 1] = pbuf[rows(zm, 1), :]
        cols = pl.ds(pl.multiple_of(yy * 512, 512), 512)
        br[h * 64 : h * 64 + 64, cols] = pbuf[pl.ds(pl.multiple_of(z * 64, 64), 64), :]
        for sign in (1, -1):
            lane = tee(sign)
            send(rs1.at[layer, h, j, lane], rr1.at[layer, h, j, lane],
                 rs_send.at[layer, h, j, lane], rs_recv.at[layer, h, j, lane], z_dev[sign])

    def combine(layer, h, dy):
        j = order.index(dy)
        for sign in (1, -1):
            lane = tee(sign)
            await_copy(rr1.at[layer, h, j, lane], rs_send.at[layer, h, j, lane], rs_recv.at[layer, h, j, lane], z_dev[-sign])
            half = slice(0, 32) if sign > 0 else slice(32, 64)
            rs2[layer, h, j, lane] = (rr1[layer, h, j, lane, half, :].astype(F32) + keep[h, j, lane]).astype(BF)
            send(rs2.at[layer, h, j, lane], rr2.at[layer, h, j, lane],
                 rs_send.at[layer, h, j, 2 + lane], rs_recv.at[layer, h, j, 2 + lane], z_dev[sign])

    def own_sum(layer, h, dy):
        j = order.index(dy)
        for sign in (1, -1):
            lane = tee(sign)
            await_copy(rr2.at[layer, h, j, lane], rs_send.at[layer, h, j, 2 + lane], rs_recv.at[layer, h, j, 2 + lane], z_dev[-sign])
        cols = pl.ds(pl.multiple_of(mod4(y + dy) * 512, 512), 512)
        a = slice(h * 64, h * 64 + 32)
        b = slice(h * 64 + 32, h * 64 + 64)
        br[a, cols] += rr2[layer, h, j, 0].astype(F32) + rr1[layer, h, j, 1, 0:32, :].astype(F32)
        br[b, cols] += rr2[layer, h, j, 1].astype(F32) + rr1[layer, h, j, 0, 32:64, :].astype(F32)

    def finish(layer, h):
        for dy in order:
            own_sum(layer, h, dy)

        def body(i, carry):
            rows = pl.ds(pl.multiple_of(h * 64 + i * 16, 16), 16)
            branch = br[rows, :]
            if layer == 0:
                m = tokv[rows, :].astype(F32) + 0.5 * rms(branch, gains[1]) + rms(mixv[rows, :].astype(F32), gains[2])
                m = m.astype(BF)
                mixed[rows, :] = m
                x_rows(1, h, z, i)[...] = rms(m.astype(F32), gains[3]).astype(BF)
            else:
                out[rows, :] = (mixed[rows, :].astype(F32) + 0.5 * rms(branch, gains[4])).astype(BF)
            return carry

        lax.fori_loop(0, 4, body, 0)
        if layer == 0:
            ag_send_own(1, h)

    own_start = True
    wait_local(0)
    for sign in (1, -1):
        send_y(0, sign, 0)
        send_x(0, sign, 0)
        send_y(0, sign, 1)
        send_x(0, sign, 1)
    own_partner(0)
    wait_local("small")
    for h in (0, 1):
        early_norm(h)
        ag_send_own(0, h)

    events = []

    def at(time, fn, *args):
        events.append((time, len(events), fn, args))

    starts = (0.0, 24.6, 36.9, 61.5)
    steps = (3.5, 1.76, 3.5, 1.76)
    for r in range(4):
        for j in range(7):
            at(2.5 + starts[r] + steps[r] * (j + 1), y_event, r, j)
            at(4.5 + starts[r] + steps[r] * (j + 1), x_event, r, j)
    at(6.1, ag_forward, 0, 0, 0)
    at(6.1, ag_forward, 0, 0, 1)
    at(11.5, ag_forward, 0, 1, 0)
    at(11.5, ag_forward, 0, 1, 1)
    at(18.9, ag_finish, 0, 0)
    at(18.9, ag_finish, 0, 1)
    for time, tasks in (
        (19.0, ((0, 0, 0), (1, 0, 0), (0, 0, 1), (1, 0, 1))),
        (20.5, ((0, -1, 0), (1, 1, 0), (0, 2, 0), (1, 2, 0))),
        (22.3, ((0, 2, 1), (1, 2, 1))),
        (24.0, ((0, 1, 0), (1, -1, 0))),
        (27.2, ((0, -1, 1), (1, 1, 1))),
        (29.2, ((0, 1, 1), (1, -1, 1))),
    ):
        for task in tasks:
            at(time, gemm, *task)
    at(30.0, hidden_early, 0)
    at(31.5, hidden_early, 1)
    for time, fn, h, dy in (
        (32.7, down, 0, 0), (33.5, down, 1, 0), (36.5, combine, 0, 0), (37.5, combine, 1, 0),
        (38.0, down, 0, 2), (38.8, down, 1, 2), (41.5, down, 0, -1), (42.0, down, 0, 1), (42.5, combine, 0, 2),
        (43.0, down, 1, -1), (43.2, combine, 1, 2), (45.0, combine, 0, -1), (45.2, down, 1, 1),
        (46.5, combine, 0, 1), (48.0, combine, 1, -1), (49.5, combine, 1, 1),
    ):
        at(time, fn, 0, h, dy)
    at(49.7, finish, 0, 0)
    at(52.5, ag_forward, 1, 0, 0)
    at(53.5, finish, 0, 1)
    at(54.0, ag_forward, 1, 0, 1)
    at(58.0, ag_forward, 1, 1, 0)
    at(59.5, ag_forward, 1, 1, 1)
    at(62.0, ag_finish, 1, 0)
    for n in range(5):
        at(66.1 + 0.7 * n, hidden_later, 0, n)
    at(69.6, ag_finish, 1, 1)
    for n in range(5):
        at(70.5 + 0.7 * n, hidden_later, 1, n)
    for time, fn, h, dy in (
        (70.0, down, 0, 0), (74.0, down, 1, 0), (74.5, combine, 0, 0), (75.0, down, 0, 2), (75.5, down, 1, 2),
        (77.0, combine, 1, 0), (78.5, down, 0, -1), (78.8, down, 0, 1), (79.0, combine, 0, 2), (79.2, down, 1, -1),
        (79.4, combine, 1, 2), (79.6, down, 1, 1), (81.0, combine, 0, -1), (82.0, combine, 0, 1),
        (83.0, combine, 1, -1), (84.0, combine, 1, 1),
    ):
        at(time, fn, 1, h, dy)
    at(86.0, finish, 1, 0)
    at(88.0, finish, 1, 1)
    for _, _, fn, args in sorted(events, key=lambda e: e[:2]):
        fn(*args)

    for r in range(4):
        for dy in (0, 1, -1, 2):
            for dp in (0, 1):
                for st in (0, 1):
                    for s in (0, 1):
                        need(r, (dy, dp, st, s))
    for copy in sent:
        copy.wait_send()


def on_device(tokens, mixer_output, en, eg, ev, ed, ep, mg, ln, lg, lv, ld, lp):
    gains = [g.reshape(1, 2048) for g in (en, ep, mg, ln, lp)]
    en, ep, mg, ln, lp = gains
    return pl.pallas_call(
        kernel,
        out_shape=jax.ShapeDtypeStruct((128, 2048), BF),
        in_specs=[pl.BlockSpec(memory_space=pl.ANY)] * 13,
        out_specs=pl.BlockSpec(memory_space=pltpu.VMEM),
        scratch_shapes=[
            pltpu.VMEM((2, 2048, 1280), BF),
            pltpu.VMEM((2, 2048, 1280), BF),
            pltpu.VMEM((2, 8, 2, 1280, 128), BF),
            pltpu.VMEM((2, 512, 2048), BF),
            pltpu.VMEM((2, 512, 1280), F32),
            pltpu.VMEM((512, 1280), BF),
            pltpu.VMEM((128, 2048), BF),
            pltpu.VMEM((128, 2048), BF),
            pltpu.VMEM((128, 2048), BF),
            pltpu.VMEM((5, 1, 2048), F32),
            pltpu.VMEM((2, 2, 4, 2, 64, 512), BF),
            pltpu.VMEM((2, 2, 4, 2, 64, 512), BF),
            pltpu.VMEM((2, 2, 4, 2, 32, 512), BF),
            pltpu.VMEM((2, 2, 4, 2, 32, 512), BF),
            pltpu.VMEM((2, 4, 2, 32, 512), F32),
            pltpu.VMEM((128, 2048), F32),
            pltpu.VMEM((256, 512), F32),
            pltpu.SemaphoreType.DMA((16,)),
            pltpu.SemaphoreType.DMA((4, 4, 7)),
            pltpu.SemaphoreType.DMA((4, 4, 7)),
            pltpu.SemaphoreType.DMA((4, 32)),
            pltpu.SemaphoreType.DMA((4, 32)),
            pltpu.SemaphoreType.DMA((2, 2, 2, 6)),
            pltpu.SemaphoreType.DMA((2, 2, 2, 6)),
            pltpu.SemaphoreType.DMA((2, 2, 4, 4)),
            pltpu.SemaphoreType.DMA((2, 2, 4, 4)),
        ],
        compiler_params=pltpu.CompilerParams(
            collective_id=0, has_side_effects=True, vmem_limit_bytes=67_000_000
        ),
    )(tokens, mixer_output, en, eg, ev, ed, ep, mg, ln, lg, lv, ld, lp)


def solution(mesh):
    placed = (
        P(("rep", "fs", "tp"), None),
        P(("rep", "fs", "tp"), None),
        P(),
        P("fs", "tp"),
        P("fs", "tp"),
        P("tp", "fs"),
        P(),
        P(),
        P(),
        P("fs", "tp"),
        P("fs", "tp"),
        P("tp", "fs"),
        P(),
    )
    return jax.shard_map(
        on_device,
        mesh=mesh,
        in_specs=placed,
        out_specs=P(("rep", "fs", "tp"), None),
        check_vma=False,
    )
```

time: 437 us -> 138 us (0.32)
  waiting for transfers between devices: 371 us -> 0 us
  Pallas kernels: 0 us -> 136 us
  matrix products: 40.1 us -> 0 us
  between operations: 13.6 us -> 0.01 us
  other arithmetic: 10.7 us -> 0 us
    all_gather x8 -> x0, waiting for transfers between devices: 311 us -> none  [the longest x4 144 us: gathered(): return lax.all_gather(part, axis, axis=dim, tiled=True)]
    pallas_call x0 -> x1, Pallas kernels: none -> 136 us  [on_device(): pl.pallas_call(kernel, out_shape=jax.ShapeDtypeStruct((128, 2048), BF), i...]
    reduce_scatter x2 -> x0, waiting for transfers between devices: 56.5 us -> none  [own_rows(): lax.psum_scatter(everything.astype(jnp.bfloat16), axis, scatter_dimension...]
    dot_general x4 -> x0, matrix products: 40.1 us -> none  [the longest x2 25 us: row_term(): return jnp.dot(rows, down_block, preferred_element_type=jnp.float32)]
    reduce_sum x5 -> x0, other arithmetic: 5.49 us -> none  [rms_scale(): jnp.mean(values * values, axis=-1, keepdims=True) + epsilon]
    convert_element_type x3 -> x0, other arithmetic: 5.14 us -> none  [the longest x1 2.13 us: on_device(): return layer_out.astype(jnp.bfloat16)]
  transfers between devices with their start and end apart: 10 -> 0, of which waited for: 10 -> 0; matrix products, arithmetic and copies ran while one was open for 4% -> 0% of each run, Pallas kernels for 0% -> 0%
where the time goes in v1:
time: 138 us
  Pallas kernels  136 us (99%)
  local copies, waits for them, and re-layouts  1.88 us (1%)
    pallas_call x1, Pallas kernels, on_device(): pl.pallas_call(kernel, out_shape=jax.ShapeDtypeStruct((128, 2048), BF), i...  136 us

profile of v1, /device:TPU:1, one launch (start us, length us, event | category | flops | bytes accessed | tf_op | source)
XLA Modules:
  0.0 137.8 jit_solution(4598502901097155360)
XLA Ops:
  0.0 135.9 %shard_map.127 = bf16[128,2048]{1,0:T(8,128)(2,1)} custom-call(bf16[128,2048]{1,0:T(8,128)(2,1)} %tok.1, bf16[128,2048]{1,0:T(8,128)(2,1)} %mix.1, f32[1,2048]{1,0:T(1,128)} %bitcast.5, bf16[128,1280]{1,0:T(8,128)(2,1)} %eg.1, bf16[128,1280]{1,0:T(8,128)(2,1)} %ev.1, bf16[1280,128]{1,0:T(8,128)(2,1)} %ed.1, f32[1,2048]{1,0:T(1,128)} %bitcast.6, ...), custom_call_target="tpu_custom_call" | custom-call | tf_op jit(solution)/shard_map/pallas_call | solution.py:466
  135.9 1.9 %copy.15 = bf16[128,2048]{1,0:T(8,128)(2,1)} copy(bf16[128,2048]{1,0:T(8,128)(2,1)} %shard_map.127) | data formatting | bytes 1048576

commit v2 on v1

v2 whole, which is shorter than its diff:
```python
import functools

import jax
import jax.numpy as jnp
from jax import lax
from jax.experimental import pallas as pl
from jax.experimental.pallas import tpu as pltpu
from jax.sharding import PartitionSpec as P

MESH = pl.DeviceIdType.MESH
EPS = 1e-06
BF = jnp.bfloat16
F32 = jnp.float32


ORDER = (
    ("en", 0), ("en", 1), ("ao", 0, 0, 0), ("ao", 0, 0, 1), ("ao", 0, 0, 2), ("ao", 0, 0, 3), ("ao", 0, 1, 0),
    ("af", 0, 0, 0), ("y", 0, 0), ("x", 0, 0), ("af", 0, 0, 1), ("ao", 0, 1, 1), ("y", 0, 1), ("x", 0, 1),
    ("ao", 0, 1, 2), ("af", 0, 1, 0), ("ao", 0, 1, 3), ("y", 0, 2), ("x", 0, 2), ("ae", 0, 0), ("af", 0, 1, 1),
    ("y", 0, 3), ("x", 0, 3), ("y", 0, 4), ("x", 0, 4), ("ae", 0, 1), ("g1", 0, 0), ("g1", 1, 0), ("g1", 0, 1),
    ("g1", 1, 1), ("g1", 0, 2), ("g1", 1, 2), ("y", 0, 5), ("x", 0, 5), ("g1", 0, 3), ("g1", 1, 3), ("g1", 0, 4),
    ("g1", 1, 4), ("y", 0, 6), ("x", 0, 6), ("g2", 0, 0), ("g2", 1, 0), ("g2", 0, 1), ("g2", 1, 1), ("g2", 0, 2),
    ("g2", 1, 2), ("y", 1, 0), ("x", 1, 0), ("g2", 0, 3), ("g2", 1, 3), ("g2", 0, 4), ("g2", 1, 4), ("y", 1, 1),
    ("x", 1, 1), ("he", 0, 0), ("he", 0, 1), ("he", 0, 2), ("he", 0, 3), ("he", 0, 4), ("d", 0, 0, (0, 0)),
    ("he", 1, 0), ("y", 1, 2), ("x", 1, 2), ("he", 1, 1), ("d", 0, 0, (0, 1)), ("he", 1, 2), ("he", 1, 3),
    ("he", 1, 4), ("y", 1, 3), ("x", 1, 3), ("d", 0, 1, (0, 0)), ("d", 0, 1, (0, 1)), ("c", 0, 0, (0, 0)),
    ("y", 1, 4), ("c", 0, 0, (0, 1)), ("x", 1, 4), ("d", 0, 0, (2, 0)), ("d", 0, 1, (2, 0)), ("c", 0, 1, (0, 0)),
    ("y", 1, 5), ("x", 1, 5), ("c", 0, 1, (0, 1)), ("y", 1, 6), ("c", 0, 0, (2, 0)), ("x", 1, 6),
    ("c", 0, 1, (2, 0)), ("d", 0, 0, (-1, 0)), ("d", 0, 0, (1, 0)), ("d", 0, 0, (2, 1)), ("d", 0, 1, (-1, 0)),
    ("d", 0, 0, (-1, 1)), ("y", 2, 0), ("d", 0, 0, (1, 1)), ("x", 2, 0), ("d", 0, 1, (1, 0)), ("c", 0, 0, (-1, 0)),
    ("c", 0, 0, (1, 0)), ("d", 0, 1, (2, 1)), ("c", 0, 0, (2, 1)), ("c", 0, 1, (-1, 0)), ("y", 2, 1),
    ("d", 0, 1, (-1, 1)), ("x", 2, 1), ("c", 0, 0, (-1, 1)), ("c", 0, 0, (1, 1)), ("d", 0, 1, (1, 1)),
    ("c", 0, 1, (1, 0)), ("c", 0, 1, (2, 1)), ("y", 2, 2), ("x", 2, 2), ("c", 0, 1, (-1, 1)), ("f", 0, 0),
    ("c", 0, 1, (1, 1)), ("ao", 1, 0, 0), ("ao", 1, 0, 1), ("ao", 1, 0, 2), ("y", 2, 3), ("x", 2, 3),
    ("ao", 1, 0, 3), ("f", 0, 1), ("ao", 1, 1, 0), ("af", 1, 0, 0), ("y", 2, 4), ("x", 2, 4), ("af", 1, 0, 1),
    ("ao", 1, 1, 1), ("y", 2, 5), ("x", 2, 5), ("ao", 1, 1, 2), ("af", 1, 1, 0), ("y", 2, 6), ("ao", 1, 1, 3),
    ("x", 2, 6), ("ae", 1, 0), ("y", 3, 0), ("x", 3, 0), ("af", 1, 1, 1), ("y", 3, 1), ("hl", 0, 0), ("x", 3, 1),
    ("hl", 0, 1), ("hl", 0, 2), ("y", 3, 2), ("x", 3, 2), ("hl", 0, 3), ("hl", 0, 4), ("y", 3, 3), ("x", 3, 3),
    ("d", 1, 0, (0, 0)), ("ae", 1, 1), ("d", 1, 0, (0, 1)), ("hl", 1, 0), ("y", 3, 4), ("hl", 1, 1), ("x", 3, 4),
    ("d", 1, 0, (2, 0)), ("hl", 1, 2), ("y", 3, 5), ("c", 1, 0, (0, 0)), ("hl", 1, 3), ("x", 3, 5),
    ("c", 1, 0, (0, 1)), ("hl", 1, 4), ("y", 3, 6), ("d", 1, 1, (0, 0)), ("x", 3, 6), ("c", 1, 0, (2, 0)),
    ("d", 1, 0, (-1, 0)), ("d", 1, 0, (1, 0)), ("d", 1, 0, (2, 1)), ("d", 1, 1, (0, 1)), ("d", 1, 0, (-1, 1)),
    ("c", 1, 1, (0, 0)), ("d", 1, 0, (1, 1)), ("c", 1, 0, (-1, 0)), ("d", 1, 1, (2, 0)), ("c", 1, 0, (1, 0)),
    ("c", 1, 0, (2, 1)), ("d", 1, 1, (-1, 0)), ("c", 1, 1, (0, 1)), ("c", 1, 0, (-1, 1)), ("d", 1, 1, (1, 0)),
    ("c", 1, 0, (1, 1)), ("d", 1, 1, (2, 1)), ("c", 1, 1, (2, 0)), ("d", 1, 1, (-1, 1)), ("d", 1, 1, (1, 1)),
    ("c", 1, 1, (-1, 0)), ("c", 1, 1, (1, 0)), ("f", 1, 0), ("c", 1, 1, (2, 1)), ("c", 1, 1, (-1, 1)),
    ("c", 1, 1, (1, 1)), ("f", 1, 1),
)


def kernel(
    tok, mix, en, eg, ev, ed, ep, mg, ln, lg, lv, ld, lp,
    out,
    gbuf, vbuf, dbuf, xbuf, acc, hbuf, tokv, mixv, mixed, gains,
    rs1, rr1, rs2, rr2, keep, br, pbuf,
    loc_sem, w_send, w_recv, p_send, p_recv, ag_send, ag_recv, rs_send, rs1_recv, rs2_recv,
):
    rep = lax.axis_index("rep")
    fs = lax.axis_index("fs")
    z = lax.axis_index("tp")
    c = lax.rem(fs, 2)
    xl = lax.rem(fs // 2, 2)
    y = fs // 4
    x = rep * 2 + xl

    def mod4(v):
        return lax.rem(v + 8, 4)

    def dev(dx=0, dy=0, dz=0, dc=0):
        nx = mod4(x + dx)
        ny = mod4(y + dy)
        nc = c if dc == 0 else 1 - c
        return (nx // 2, (ny * 2 + lax.rem(nx, 2)) * 2 + nc, mod4(z + dz))

    y_dev = {1: dev(dy=1), -1: dev(dy=-1)}
    x_dev = {1: dev(dx=1), -1: dev(dx=-1)}
    z_dev = {1: dev(dz=1), -1: dev(dz=-1)}
    partner = dev(dc=1)
    everyone = [y_dev[1], y_dev[-1], x_dev[1], x_dev[-1], z_dev[1], z_dev[-1], partner]
    zp, zm, zo = mod4(z + 1), mod4(z - 1), mod4(z + 2)

    def blk_of(dy, dp):
        return mod4(y + dy) * 2 + (xl if dp == 0 else 1 - xl)

    blocks = {(dy, dp): blk_of(dy, dp) for dy in (0, 1, -1, 2) for dp in (0, 1)}

    def unit(r, content, core):
        dy, dp, st, s = content
        blk = blocks[(dy, dp)]
        layer = r // 2
        if r % 2 == 0:
            buf = gbuf if st == 0 else vbuf
            row = pl.multiple_of(blk * 256 + core * 128 + s * 64, 64)
            return buf.at[layer, pl.ds(row, 64), :]
        return dbuf.at[layer, blk, core, pl.ds(st * 640 + s * 320, 320), :]

    def unit_id(content):
        dy, dp, st, s = content
        return (((dy % 4) * 2 + dp) * 2 + st) * 2 + s

    def send(src, dst, send_sem, recv_sem, target):
        pltpu.make_async_remote_copy(src, dst, send_sem, recv_sem, device_id=target, device_id_type=MESH).start()

    def await_bytes(ref, sem):
        pltpu.make_async_copy(ref, ref, sem).wait()

    def units(r, n):
        return gbuf.at[0, pl.ds(0, n * (64 if r % 2 == 0 else 32)), :]

    def tee(sign):
        return 0 if sign > 0 else 1

    def y_recv_content(sign, k):
        t = tee(sign)
        return [(-sign, 0, t, 0), (-sign, 0, t, 1), (2, 0, t, 0), (2, 0, t, 1),
                (-sign, 0, 1 - t, 0), (-sign, 0, 1 - t, 1), (-sign, 1, 1 - t, 1)][k]

    def y_send_content(sign, k):
        t = tee(sign)
        return [(0, 0, t, 0), (0, 0, t, 1), (-sign, 0, t, 0), (-sign, 0, t, 1),
                (0, 0, 1 - t, 0), (0, 0, 1 - t, 1), (0, 1, 1 - t, 1)][k]

    def x_content(sign, k, dp):
        t = tee(sign)
        return [(0, dp, t, 0), (0, dp, t, 1), (-sign, dp, t, 0), (-sign, dp, t, 1), (2, dp, t, 0),
                (2, dp, t, 1), (sign, dp, t, 0)][k]

    have = set()
    partner_have = set()

    def group_of(r, content):
        dy, dp, st, s = content
        if r == 2:
            return 19
        if r == 0:
            last = 1 if st == 0 else -1
            return 0 if dy in (0, -last) else (1 if dy == 2 else 2)
        return 3 + (r // 2) * 8 + (dy % 4) * 2 + dp

    def send_y(r, sign, k):
        content = y_send_content(sign, k)
        assert (r, content) in have
        ref = unit(r, content, c)
        send(ref, ref, w_send.at[r], w_recv.at[r, 0, k], y_dev[sign])

    def send_x(r, sign, k):
        content = x_content(sign, k, 0)
        assert (r, content) in have
        ref = unit(r, content, c)
        send(ref, ref, w_send.at[r], w_recv.at[r, 1, k], x_dev[sign])

    def send_partner(r, content):
        ref = unit(r, content, c)
        send(ref, ref, p_send.at[r], p_recv.at[group_of(r, content)], partner)

    every = [(dy, dp, st, s) for dy in (0, 1, -1, 2) for dp in (0, 1) for st in (0, 1) for s in (0, 1)]

    def need(r, group):
        members = [content for content in every if group_of(r, content) == group]
        assert all((r, content) in have for content in members), (r, group)
        if group not in partner_have:
            partner_have.add(group)
            await_bytes(units(r, len(members)), p_recv.at[group])

    def own_y(r):
        wait_local(r)
        for sign in (1, -1):
            send_y(r, sign, 0)
            send_y(r, sign, 1)

    def own_x(r):
        for sign in (1, -1):
            send_x(r, sign, 0)
            send_x(r, sign, 1)

    def own_partner(r):
        for st in (0, 1):
            for s in (0, 1):
                send_partner(r, (0, 0, st, s))

    def y_event(r, j):
        await_bytes(units(r, 2), w_recv.at[r, 0, j])
        for sign in (1, -1):
            have.add((r, y_recv_content(sign, j)))
        for sign in (1, -1):
            if j == 0:
                send_x(r, sign, 2)
                send_y(r, sign, 2)
            elif j == 1:
                send_x(r, sign, 3)
                send_y(r, sign, 3)
                send_y(r, sign, 4)
                send_y(r, sign, 5)
            elif j == 2:
                send_x(r, sign, 4)
            elif j == 3:
                send_x(r, sign, 5)
            elif j == 4:
                send_x(r, -sign, 6)
        if r < 3 and j == 3:
            own_y(r + 1)
        if r < 3 and j == 5:
            own_x(r + 1)
        for sign in (1, -1):
            send_partner(r, y_recv_content(sign, j))
        if r < 3 and j == 3:
            own_partner(r + 1)

    def x_event(r, j):
        await_bytes(units(r, 2), w_recv.at[r, 1, j])
        for sign in (1, -1):
            have.add((r, x_content(sign, j, 1)))
        for sign in (1, -1):
            if j == 1:
                send_y(r, sign, 6)
            send_partner(r, x_content(sign, j, 1))

    own = pl.multiple_of(blocks[(0, 0)] * 256 + c * 128, 128)
    weights = {
        0: [(eg, gbuf.at[0, pl.ds(own, 128), :]), (ev, vbuf.at[0, pl.ds(own, 128), :])],
        1: [(ed, dbuf.at[0, blocks[(0, 0)], c])],
        2: [(lg, gbuf.at[1, pl.ds(own, 128), :]), (lv, vbuf.at[1, pl.ds(own, 128), :])],
        3: [(ld, dbuf.at[1, blocks[(0, 0)], c])],
    }
    norms = [(g, gains.at[i]) for i, g in enumerate((en, ep, mg, ln, lp))]
    for i, pairs in enumerate((weights[0], [(tok, tokv)], norms, weights[1], weights[2], weights[3], [(mix, mixv)])):
        for src, dst in pairs:
            pltpu.make_async_copy(src, dst, loc_sem.at[i]).start()

    def wait_local(r):
        await_bytes(units(r, 4), loc_sem.at[(0, 3, 4, 5)[r]])
        for st in (0, 1):
            for s in (0, 1):
                have.add((r, (0, 0, st, s)))

    barrier = pltpu.get_barrier_semaphore()
    for other in everyone:
        pl.semaphore_signal(barrier, inc=1, device_id=other, device_id_type=MESH)
    pl.semaphore_wait(barrier, len(everyone))

    def x_rows(layer, h, zz, u, n=16):
        row = pl.multiple_of(h * 256 + zz * 64 + u * 16, 16)
        return xbuf.at[layer, pl.ds(row, n), :]

    def ag_own(layer, h, u):
        for sign in (1, -1):
            v = u if sign > 0 else (u + 2) % 4
            ref = x_rows(layer, h, z, v)
            send(ref, ref, ag_send.at[layer], ag_recv.at[layer, h, min(u, 2)], z_dev[sign])

    def ag_forward(layer, h, u):
        await_bytes(xbuf.at[0, pl.ds(0, 32), :], ag_recv.at[layer, h, u])
        for sign in (1, -1):
            v = u if sign > 0 else u + 2
            ref = x_rows(layer, h, zm if sign > 0 else zp, v)
            send(ref, ref, ag_send.at[layer], ag_recv.at[layer, h, 2], z_dev[sign])

    def ag_finish(layer, h):
        await_bytes(xbuf.at[0, pl.ds(0, 128), :], ag_recv.at[layer, h, 2])

    def rms(v, gain):
        return v * lax.rsqrt(jnp.mean(v * v, axis=-1, keepdims=True) + EPS) * gain

    def early_norm(h):
        def body(i, carry):
            rows = pl.ds(pl.multiple_of(h * 64 + i * 16, 16), 16)
            v = rms(tokv[rows, :].astype(F32), gains[0])
            x_rows(0, h, z, i)[...] = v.astype(BF)
            return carry

        lax.fori_loop(0, 4, body, 0)

    def dot_rows(st, rows, dy, cols):
        base = pl.multiple_of(mod4(y + dy) * 512, 512)
        w = gbuf if st == 0 else vbuf
        return jnp.dot(xbuf[0, rows, pl.ds(base, 512)], w[0, pl.ds(base, 512), cols], preferred_element_type=F32)

    whole = slice(0, 512)

    def tile(n):
        return slice(n * 256, n * 256 + 256)

    def gemm1(st, n):
        need(0, 0)
        acc[st, :, tile(n)] = dot_rows(st, whole, 0, tile(n)) + dot_rows(st, whole, -1 if st == 0 else 1, tile(n))

    def gemm2(st, n):
        need(0, 1)
        acc[st, :, tile(n)] += dot_rows(st, whole, 2, tile(n))

    def silu_mul(g, v):
        return (g * (1.0 / (1.0 + jnp.exp(-g))) * v).astype(BF)

    def hidden_early(h, n):
        need(0, 2)
        rows = slice(h * 256, h * 256 + 256)
        g = acc[0, rows, tile(n)] + dot_rows(0, rows, 1, tile(n))
        v = acc[1, rows, tile(n)] + dot_rows(1, rows, -1, tile(n))
        hbuf[rows, tile(n)] = silu_mul(g, v)

    def hidden_later(h, n):
        need(2, 19)
        rows = slice(h * 256, h * 256 + 256)
        cols = slice(n * 256, n * 256 + 256)
        xs = xbuf[1, rows, :]
        g = jnp.dot(xs, gbuf[1, :, cols], preferred_element_type=F32)
        v = jnp.dot(xs, vbuf[1, :, cols], preferred_element_type=F32)
        hbuf[rows, cols] = silu_mul(g, v)

    chunks = ((0, 0), (0, 1), (2, 0), (-1, 0), (1, 0), (2, 1), (-1, 1), (1, 1))

    def down(layer, h, chunk):
        r = 2 * layer + 1
        dy, dp = chunk
        need(r, group_of(r, (dy, dp, 0, 0)))
        j = chunks.index(chunk)
        blk = blocks[chunk]
        w = jnp.concatenate([dbuf[layer, blk, 0], dbuf[layer, blk, 1]], axis=1)
        pbuf[...] = jnp.dot(hbuf[h * 256 : h * 256 + 256, :], w, preferred_element_type=F32)

        def rows(zz, half):
            return pl.ds(pl.multiple_of(zz * 64 + half * 32, 32), 32)

        rs1[layer, h, j, 0, 0:32, :] = pbuf[rows(zo, 0), :].astype(BF)
        rs1[layer, h, j, 0, 32:64, :] = pbuf[rows(zp, 1), :].astype(BF)
        rs1[layer, h, j, 1, 0:32, :] = pbuf[rows(zm, 0), :].astype(BF)
        rs1[layer, h, j, 1, 32:64, :] = pbuf[rows(zo, 1), :].astype(BF)
        keep[h, j, 0] = pbuf[rows(zp, 0), :]
        keep[h, j, 1] = pbuf[rows(zm, 1), :]
        cols = pl.ds(pl.multiple_of(blk * 256, 256), 256)
        br[h * 64 : h * 64 + 64, cols] = pbuf[pl.ds(pl.multiple_of(z * 64, 64), 64), :]
        for sign in (1, -1):
            lane = tee(sign)
            send(rs1.at[layer, h, j, lane], rr1.at[layer, h, j, lane], rs_send.at[0], rs1_recv.at[layer, h, j], z_dev[sign])

    def combine(layer, h, chunk):
        j = chunks.index(chunk)
        await_bytes(rr1.at[layer, h, j], rs1_recv.at[layer, h, j])
        for sign in (1, -1):
            lane = tee(sign)
            half = slice(0, 32) if sign > 0 else slice(32, 64)
            rs2[layer, h, j, lane] = (rr1[layer, h, j, lane, half, :].astype(F32) + keep[h, j, lane]).astype(BF)
        for sign in (1, -1):
            lane = tee(sign)
            send(rs2.at[layer, h, j, lane], rr2.at[layer, h, j, lane], rs_send.at[1], rs2_recv.at[layer, h], z_dev[sign])

    def finish(layer, h):
        await_bytes(rr2.at[layer, h], rs2_recv.at[layer, h])
        a = slice(h * 64, h * 64 + 32)
        b = slice(h * 64 + 32, h * 64 + 64)
        for j, chunk in enumerate(chunks):
            cols = pl.ds(pl.multiple_of(blocks[chunk] * 256, 256), 256)
            br[a, cols] += rr2[layer, h, j, 0].astype(F32) + rr1[layer, h, j, 1, 0:32, :].astype(F32)
            br[b, cols] += rr2[layer, h, j, 1].astype(F32) + rr1[layer, h, j, 0, 32:64, :].astype(F32)

        def body(i, carry):
            rows = pl.ds(pl.multiple_of(h * 64 + i * 16, 16), 16)
            branch = br[rows, :]
            if layer == 0:
                m = tokv[rows, :].astype(F32) + 0.5 * rms(branch, gains[1]) + rms(mixv[rows, :].astype(F32), gains[2])
                m = m.astype(BF)
                mixed[rows, :] = m
                x_rows(1, h, z, i)[...] = rms(m.astype(F32), gains[3]).astype(BF)
            else:
                out[rows, :] = (mixed[rows, :].astype(F32) + 0.5 * rms(branch, gains[4])).astype(BF)
            return carry

        lax.fori_loop(0, 4, body, 0)

    wait_local(0)
    for sign in (1, -1):
        send_y(0, sign, 0)
        send_x(0, sign, 0)
        send_y(0, sign, 1)
        send_x(0, sign, 1)
    own_partner(0)
    await_bytes(tokv, loc_sem.at[1])
    await_bytes(gains, loc_sem.at[2])
    await_bytes(mixv, loc_sem.at[6])
    tasks = dict(
        y=y_event, x=x_event, en=early_norm, ao=ag_own, af=ag_forward, ae=ag_finish, g1=gemm1, g2=gemm2,
        he=hidden_early, hl=hidden_later, d=down, c=combine, f=finish,
    )
    for name, *args in ORDER:
        fn = tasks[name]
        fn(*args)

    for r in range(4):
        await_bytes(units(r, 28), w_send.at[r])
        await_bytes(units(r, 32), p_send.at[r])
    for layer in (0, 1):
        await_bytes(xbuf.at[0, pl.ds(0, 384), :], ag_send.at[layer])
    await_bytes(rs1, rs_send.at[0])
    await_bytes(rs2, rs_send.at[1])


def on_device(tokens, mixer_output, en, eg, ev, ed, ep, mg, ln, lg, lv, ld, lp):
    gains = [g.reshape(1, 2048) for g in (en, ep, mg, ln, lp)]
    en, ep, mg, ln, lp = gains
    return pl.pallas_call(
        kernel,
        out_shape=jax.ShapeDtypeStruct((128, 2048), BF),
        in_specs=[pl.BlockSpec(memory_space=pl.ANY)] * 13,
        out_specs=pl.BlockSpec(memory_space=pltpu.VMEM),
        scratch_shapes=[
            pltpu.VMEM((2, 2048, 1280), BF),
            pltpu.VMEM((2, 2048, 1280), BF),
            pltpu.VMEM((2, 8, 2, 1280, 128), BF),
            pltpu.VMEM((2, 512, 2048), BF),
            pltpu.VMEM((2, 512, 1280), F32),
            pltpu.VMEM((512, 1280), BF),
            pltpu.VMEM((128, 2048), BF),
            pltpu.VMEM((128, 2048), BF),
            pltpu.VMEM((128, 2048), BF),
            pltpu.VMEM((5, 1, 2048), F32),
            pltpu.VMEM((2, 2, 8, 2, 64, 256), BF),
            pltpu.VMEM((2, 2, 8, 2, 64, 256), BF),
            pltpu.VMEM((2, 2, 8, 2, 32, 256), BF),
            pltpu.VMEM((2, 2, 8, 2, 32, 256), BF),
            pltpu.VMEM((2, 8, 2, 32, 256), F32),
            pltpu.VMEM((128, 2048), F32),
            pltpu.VMEM((256, 256), F32),
            pltpu.SemaphoreType.DMA((7,)),
            pltpu.SemaphoreType.DMA((4,)),
            pltpu.SemaphoreType.DMA((4, 2, 7)),
            pltpu.SemaphoreType.DMA((4,)),
            pltpu.SemaphoreType.DMA((20,)),
            pltpu.SemaphoreType.DMA((2,)),
            pltpu.SemaphoreType.DMA((2, 2, 3)),
            pltpu.SemaphoreType.DMA((2,)),
            pltpu.SemaphoreType.DMA((2, 2, 8)),
            pltpu.SemaphoreType.DMA((2, 2)),
        ],
        compiler_params=pltpu.CompilerParams(
            collective_id=0, has_side_effects=True, vmem_limit_bytes=67_000_000
        ),
    )(tokens, mixer_output, en, eg, ev, ed, ep, mg, ln, lg, lv, ld, lp)


def solution(mesh):
    placed = (
        P(("rep", "fs", "tp"), None),
        P(("rep", "fs", "tp"), None),
        P(),
        P("fs", "tp"),
        P("fs", "tp"),
        P("tp", "fs"),
        P(),
        P(),
        P(),
        P("fs", "tp"),
        P("fs", "tp"),
        P("tp", "fs"),
        P(),
    )
    return jax.shard_map(
        on_device,
        mesh=mesh,
        in_specs=placed,
        out_specs=P(("rep", "fs", "tp"), None),
        check_vma=False,
    )
```

time: 138 us -> 112 us (0.81); the launches traced: 138 us -> 109 us
  Pallas kernels: 136 us -> 107 us
    pallas_call x1, Pallas kernels: 136 us -> 107 us  [on_device(): pl.pallas_call(kernel, out_shape=jax.ShapeDtypeStruct((128, 2048), BF), i...]
where the time goes in v2:
time: 112 us; the launch traced here: 109 us
  Pallas kernels  107 us (96%)
  local copies, waits for them, and re-layouts  1.88 us (2%)
    pallas_call x1, Pallas kernels, on_device(): pl.pallas_call(kernel, out_shape=jax.ShapeDtypeStruct((128, 2048), BF), i...  107 us

profile of v2, /device:TPU:1, one launch (start us, length us, event | category | flops | bytes accessed | tf_op | source)
XLA Modules:
  0.0 109.4 jit_solution(5249339211537006175)
XLA Ops:
  0.0 107.5 %shard_map.127 = bf16[128,2048]{1,0:T(8,128)(2,1)} custom-call(bf16[128,2048]{1,0:T(8,128)(2,1)} %tok.1, bf16[128,2048]{1,0:T(8,128)(2,1)} %mix.1, f32[1,2048]{1,0:T(1,128)} %bitcast.5, bf16[128,1280]{1,0:T(8,128)(2,1)} %eg.1, bf16[128,1280]{1,0:T(8,128)(2,1)} %ev.1, bf16[1280,128]{1,0:T(8,128)(2,1)} %ed.1, f32[1,2048]{1,0:T(1,128)} %bitcast.6, ...), custom_call_target="tpu_custom_call" | custom-call | tf_op jit(solution)/shard_map/pallas_call | solution.py:400
  107.5 1.9 %copy.15 = bf16[128,2048]{1,0:T(8,128)(2,1)} copy(bf16[128,2048]{1,0:T(8,128)(2,1)} %shard_map.127) | data formatting | bytes 1048576

commit v3 on v2

--- a/solution.py
+++ b/solution.py
@@ -14,38 +14,39 @@
 
 
 ORDER = (
-    ("en", 0), ("en", 1), ("ao", 0, 0, 0), ("ao", 0, 0, 1), ("ao", 0, 0, 2), ("ao", 0, 0, 3), ("ao", 0, 1, 0),
-    ("af", 0, 0, 0), ("y", 0, 0), ("x", 0, 0), ("af", 0, 0, 1), ("ao", 0, 1, 1), ("y", 0, 1), ("x", 0, 1),
-    ("ao", 0, 1, 2), ("af", 0, 1, 0), ("ao", 0, 1, 3), ("y", 0, 2), ("x", 0, 2), ("ae", 0, 0), ("af", 0, 1, 1),
-    ("y", 0, 3), ("x", 0, 3), ("y", 0, 4), ("x", 0, 4), ("ae", 0, 1), ("g1", 0, 0), ("g1", 1, 0), ("g1", 0, 1),
-    ("g1", 1, 1), ("g1", 0, 2), ("g1", 1, 2), ("y", 0, 5), ("x", 0, 5), ("g1", 0, 3), ("g1", 1, 3), ("g1", 0, 4),
-    ("g1", 1, 4), ("y", 0, 6), ("x", 0, 6), ("g2", 0, 0), ("g2", 1, 0), ("g2", 0, 1), ("g2", 1, 1), ("g2", 0, 2),
-    ("g2", 1, 2), ("y", 1, 0), ("x", 1, 0), ("g2", 0, 3), ("g2", 1, 3), ("g2", 0, 4), ("g2", 1, 4), ("y", 1, 1),
-    ("x", 1, 1), ("he", 0, 0), ("he", 0, 1), ("he", 0, 2), ("he", 0, 3), ("he", 0, 4), ("d", 0, 0, (0, 0)),
-    ("he", 1, 0), ("y", 1, 2), ("x", 1, 2), ("he", 1, 1), ("d", 0, 0, (0, 1)), ("he", 1, 2), ("he", 1, 3),
-    ("he", 1, 4), ("y", 1, 3), ("x", 1, 3), ("d", 0, 1, (0, 0)), ("d", 0, 1, (0, 1)), ("c", 0, 0, (0, 0)),
-    ("y", 1, 4), ("c", 0, 0, (0, 1)), ("x", 1, 4), ("d", 0, 0, (2, 0)), ("d", 0, 1, (2, 0)), ("c", 0, 1, (0, 0)),
-    ("y", 1, 5), ("x", 1, 5), ("c", 0, 1, (0, 1)), ("y", 1, 6), ("c", 0, 0, (2, 0)), ("x", 1, 6),
-    ("c", 0, 1, (2, 0)), ("d", 0, 0, (-1, 0)), ("d", 0, 0, (1, 0)), ("d", 0, 0, (2, 1)), ("d", 0, 1, (-1, 0)),
-    ("d", 0, 0, (-1, 1)), ("y", 2, 0), ("d", 0, 0, (1, 1)), ("x", 2, 0), ("d", 0, 1, (1, 0)), ("c", 0, 0, (-1, 0)),
-    ("c", 0, 0, (1, 0)), ("d", 0, 1, (2, 1)), ("c", 0, 0, (2, 1)), ("c", 0, 1, (-1, 0)), ("y", 2, 1),
-    ("d", 0, 1, (-1, 1)), ("x", 2, 1), ("c", 0, 0, (-1, 1)), ("c", 0, 0, (1, 1)), ("d", 0, 1, (1, 1)),
-    ("c", 0, 1, (1, 0)), ("c", 0, 1, (2, 1)), ("y", 2, 2), ("x", 2, 2), ("c", 0, 1, (-1, 1)), ("f", 0, 0),
-    ("c", 0, 1, (1, 1)), ("ao", 1, 0, 0), ("ao", 1, 0, 1), ("ao", 1, 0, 2), ("y", 2, 3), ("x", 2, 3),
-    ("ao", 1, 0, 3), ("f", 0, 1), ("ao", 1, 1, 0), ("af", 1, 0, 0), ("y", 2, 4), ("x", 2, 4), ("af", 1, 0, 1),
-    ("ao", 1, 1, 1), ("y", 2, 5), ("x", 2, 5), ("ao", 1, 1, 2), ("af", 1, 1, 0), ("y", 2, 6), ("ao", 1, 1, 3),
-    ("x", 2, 6), ("ae", 1, 0), ("y", 3, 0), ("x", 3, 0), ("af", 1, 1, 1), ("y", 3, 1), ("hl", 0, 0), ("x", 3, 1),
-    ("hl", 0, 1), ("hl", 0, 2), ("y", 3, 2), ("x", 3, 2), ("hl", 0, 3), ("hl", 0, 4), ("y", 3, 3), ("x", 3, 3),
-    ("d", 1, 0, (0, 0)), ("ae", 1, 1), ("d", 1, 0, (0, 1)), ("hl", 1, 0), ("y", 3, 4), ("hl", 1, 1), ("x", 3, 4),
-    ("d", 1, 0, (2, 0)), ("hl", 1, 2), ("y", 3, 5), ("c", 1, 0, (0, 0)), ("hl", 1, 3), ("x", 3, 5),
-    ("c", 1, 0, (0, 1)), ("hl", 1, 4), ("y", 3, 6), ("d", 1, 1, (0, 0)), ("x", 3, 6), ("c", 1, 0, (2, 0)),
-    ("d", 1, 0, (-1, 0)), ("d", 1, 0, (1, 0)), ("d", 1, 0, (2, 1)), ("d", 1, 1, (0, 1)), ("d", 1, 0, (-1, 1)),
-    ("c", 1, 1, (0, 0)), ("d", 1, 0, (1, 1)), ("c", 1, 0, (-1, 0)), ("d", 1, 1, (2, 0)), ("c", 1, 0, (1, 0)),
-    ("c", 1, 0, (2, 1)), ("d", 1, 1, (-1, 0)), ("c", 1, 1, (0, 1)), ("c", 1, 0, (-1, 1)), ("d", 1, 1, (1, 0)),
-    ("c", 1, 0, (1, 1)), ("d", 1, 1, (2, 1)), ("c", 1, 1, (2, 0)), ("d", 1, 1, (-1, 1)), ("d", 1, 1, (1, 1)),
-    ("c", 1, 1, (-1, 0)), ("c", 1, 1, (1, 0)), ("f", 1, 0), ("c", 1, 1, (2, 1)), ("c", 1, 1, (-1, 1)),
-    ("c", 1, 1, (1, 1)), ("f", 1, 1),
+    ("en", 0), ("en", 1), ("ao", 0, 1, 0), ("ao", 0, 1, 1), ("ao", 0, 1, 2), ("ao", 0, 1, 3), ("ao", 0, 0, 0),
+    ("ao", 0, 0, 1), ("af", 0, 1, 0), ("y", 0, 0), ("x", 0, 0), ("af", 0, 1, 1), ("ao", 0, 0, 2), ("y", 0, 1),
+    ("x", 0, 1), ("ao", 0, 0, 3), ("af", 0, 0, 0), ("af", 0, 0, 1), ("y", 0, 2), ("x", 0, 2), ("ae", 0, 1),
+    ("y", 0, 3), ("x", 0, 3), ("y", 0, 4), ("x", 0, 4), ("ae", 0, 0), ("g1", 0, 1), ("g1", 0, 4), ("g1", 1, 4),
+    ("g1", 1, 2), ("y", 0, 5), ("x", 0, 5), ("g1", 0, 3), ("g1", 0, 0), ("g1", 1, 1), ("g1", 0, 2), ("g1", 1, 3),
+    ("g1", 1, 0), ("y", 0, 6), ("x", 0, 6), ("y", 1, 0), ("x", 1, 0), ("y", 1, 1), ("x", 1, 1), ("he", 1, 2),
+    ("he", 0, 4), ("he", 0, 0), ("y", 1, 2), ("he", 0, 2), ("he", 0, 1), ("x", 1, 2), ("he", 1, 4), ("y", 1, 3),
+    ("he", 1, 0), ("he", 0, 3), ("d", 0, 0, (0, 0)), ("x", 1, 3), ("d", 0, 0, (0, 1)), ("y", 1, 4), ("he", 1, 3),
+    ("he", 1, 1), ("d", 0, 1, (0, 0)), ("x", 1, 4), ("y", 1, 5), ("d", 0, 1, (0, 1)), ("x", 1, 5),
+    ("c", 0, 0, (0, 0)), ("y", 1, 6), ("d", 0, 0, (2, 0)), ("c", 0, 0, (0, 1)), ("d", 0, 1, (2, 0)), ("x", 1, 6),
+    ("d", 0, 0, (1, 0)), ("d", 0, 0, (-1, 0)), ("c", 0, 1, (0, 1)), ("d", 0, 0, (1, 1)), ("d", 0, 0, (-1, 1)),
+    ("d", 0, 0, (2, 1)), ("y", 2, 0), ("c", 0, 0, (2, 0)), ("c", 0, 1, (0, 0)), ("x", 2, 0), ("d", 0, 1, (2, 1)),
+    ("c", 0, 1, (2, 0)), ("c", 0, 0, (1, 0)), ("d", 0, 1, (-1, 1)), ("y", 2, 1), ("c", 0, 0, (-1, 0)),
+    ("d", 0, 1, (-1, 0)), ("c", 0, 0, (1, 1)), ("x", 2, 1), ("c", 0, 0, (-1, 1)), ("d", 0, 1, (1, 1)),
+    ("c", 0, 0, (2, 1)), ("d", 0, 1, (1, 0)), ("y", 2, 2), ("c", 0, 1, (2, 1)), ("x", 2, 2), ("c", 0, 1, (-1, 1)),
+    ("c", 0, 1, (-1, 0)), ("y", 2, 3), ("c", 0, 1, (1, 1)), ("f", 0, 0), ("x", 2, 3), ("ao", 1, 0, 0),
+    ("ao", 1, 0, 1), ("ao", 1, 0, 2), ("c", 0, 1, (1, 0)), ("ao", 1, 0, 3), ("y", 2, 4), ("x", 2, 4),
+    ("af", 1, 0, 0), ("y", 2, 5), ("af", 1, 0, 1), ("x", 2, 5), ("f", 0, 1), ("ao", 1, 1, 0), ("ao", 1, 1, 1),
+    ("ao", 1, 1, 2), ("y", 2, 6), ("ao", 1, 1, 3), ("x", 2, 6), ("y", 3, 0), ("ae", 1, 0), ("x", 3, 0),
+    ("y", 3, 1), ("af", 1, 1, 0), ("hl", 0, 4), ("hl", 0, 2), ("x", 3, 1), ("y", 3, 2), ("af", 1, 1, 1),
+    ("hl", 0, 1), ("hl", 0, 0), ("x", 3, 2), ("y", 3, 3), ("hl", 0, 3), ("d", 1, 0, (0, 0)), ("x", 3, 3),
+    ("d", 1, 0, (0, 1)), ("y", 3, 4), ("x", 3, 4), ("y", 3, 5), ("ae", 1, 1), ("hl", 1, 4), ("d", 1, 0, (2, 0)),
+    ("x", 3, 5), ("y", 3, 6), ("hl", 1, 2), ("c", 1, 0, (0, 1)), ("d", 1, 0, (1, 0)), ("x", 3, 6),
+    ("d", 1, 0, (-1, 0)), ("c", 1, 0, (0, 0)), ("hl", 1, 0), ("d", 1, 0, (-1, 1)), ("d", 1, 0, (1, 1)),
+    ("c", 1, 0, (2, 0)), ("hl", 1, 1), ("d", 1, 0, (2, 1)), ("c", 1, 0, (1, 0)), ("hl", 1, 3),
+    ("c", 1, 0, (-1, 0)), ("d", 1, 1, (2, 1)), ("d", 1, 1, (-1, 1)), ("d", 1, 1, (1, 0)), ("d", 1, 1, (0, 1)),
+    ("d", 1, 1, (2, 0)), ("d", 1, 1, (0, 0)), ("d", 1, 1, (1, 1)), ("d", 1, 1, (-1, 0)), ("c", 1, 1, (2, 1)),
+    ("c", 1, 0, (-1, 1)), ("c", 1, 0, (2, 1)), ("c", 1, 0, (1, 1)), ("c", 1, 1, (-1, 1)), ("c", 1, 1, (1, 0)),
+    ("c", 1, 1, (0, 1)), ("c", 1, 1, (2, 0)), ("c", 1, 1, (0, 0)), ("c", 1, 1, (1, 1)), ("c", 1, 1, (-1, 0)),
+    ("f", 1, 0), ("f", 1, 1),
 )
+OWN_Y_AT = 3
+OWN_X_AT = 4
 
 
 def kernel(
@@ -112,18 +113,18 @@
 
     def y_recv_content(sign, k):
         t = tee(sign)
-        return [(-sign, 0, t, 0), (-sign, 0, t, 1), (2, 0, t, 0), (2, 0, t, 1),
-                (-sign, 0, 1 - t, 0), (-sign, 0, 1 - t, 1), (-sign, 1, 1 - t, 1)][k]
+        return [(-sign, 0, t, 0), (-sign, 0, t, 1), (-sign, 0, 1 - t, 0), (2, 0, t, 0), (2, 0, t, 1),
+                (-sign, 0, 1 - t, 1), (-sign, 1, 1 - t, 1)][k]
 
     def y_send_content(sign, k):
         t = tee(sign)
-        return [(0, 0, t, 0), (0, 0, t, 1), (-sign, 0, t, 0), (-sign, 0, t, 1),
-                (0, 0, 1 - t, 0), (0, 0, 1 - t, 1), (0, 1, 1 - t, 1)][k]
+        return [(0, 0, t, 0), (0, 0, t, 1), (0, 0, 1 - t, 0), (-sign, 0, t, 0), (-sign, 0, t, 1),
+                (0, 0, 1 - t, 1), (0, 1, 1 - t, 1)][k]
 
     def x_content(sign, k, dp):
         t = tee(sign)
-        return [(0, dp, t, 0), (0, dp, t, 1), (-sign, dp, t, 0), (-sign, dp, t, 1), (2, dp, t, 0),
-                (2, dp, t, 1), (sign, dp, t, 0)][k]
+        return [(0, dp, t, 0), (0, dp, t, 1), (-sign, dp, t, 0), (-sign, dp, t, 1), (sign, dp, t, 0),
+                (2, dp, t, 0), (2, dp, t, 1)][k]
 
     have = set()
     partner_have = set()
@@ -131,11 +132,10 @@
     def group_of(r, content):
         dy, dp, st, s = content
         if r == 2:
-            return 19
+            return 18
         if r == 0:
-            last = 1 if st == 0 else -1
-            return 0 if dy in (0, -last) else (1 if dy == 2 else 2)
-        return 3 + (r // 2) * 8 + (dy % 4) * 2 + dp
+            return 0 if dy in (0, -1 if st == 0 else 1) else 1
+        return 2 + (r // 2) * 8 + (dy % 4) * 2 + dp
 
     def send_y(r, sign, k):
         content = y_send_content(sign, k)
@@ -165,8 +165,8 @@
     def own_y(r):
         wait_local(r)
         for sign in (1, -1):
-            send_y(r, sign, 0)
-            send_y(r, sign, 1)
+            for k in (0, 1, 2):
+                send_y(r, sign, k)
 
     def own_x(r):
         for sign in (1, -1):
@@ -185,25 +185,24 @@
         for sign in (1, -1):
             if j == 0:
                 send_x(r, sign, 2)
-                send_y(r, sign, 2)
+                send_y(r, sign, 3)
             elif j == 1:
                 send_x(r, sign, 3)
-                send_y(r, sign, 3)
                 send_y(r, sign, 4)
                 send_y(r, sign, 5)
             elif j == 2:
-                send_x(r, sign, 4)
+                send_x(r, -sign, 4)
             elif j == 3:
                 send_x(r, sign, 5)
             elif j == 4:
-                send_x(r, -sign, 6)
-        if r < 3 and j == 3:
+                send_x(r, sign, 6)
+        if r < 3 and j == OWN_Y_AT:
             own_y(r + 1)
-        if r < 3 and j == 5:
+        if r < 3 and j == OWN_X_AT:
             own_x(r + 1)
         for sign in (1, -1):
             send_partner(r, y_recv_content(sign, j))
-        if r < 3 and j == 3:
+        if r < 3 and j == OWN_Y_AT:
             own_partner(r + 1)
 
     def x_event(r, j):
@@ -284,22 +283,18 @@
         need(0, 0)
         acc[st, :, tile(n)] = dot_rows(st, whole, 0, tile(n)) + dot_rows(st, whole, -1 if st == 0 else 1, tile(n))
 
-    def gemm2(st, n):
-        need(0, 1)
-        acc[st, :, tile(n)] += dot_rows(st, whole, 2, tile(n))
-
     def silu_mul(g, v):
         return (g * (1.0 / (1.0 + jnp.exp(-g))) * v).astype(BF)
 
     def hidden_early(h, n):
-        need(0, 2)
+        need(0, 1)
         rows = slice(h * 256, h * 256 + 256)
-        g = acc[0, rows, tile(n)] + dot_rows(0, rows, 1, tile(n))
-        v = acc[1, rows, tile(n)] + dot_rows(1, rows, -1, tile(n))
+        g = acc[0, rows, tile(n)] + dot_rows(0, rows, 2, tile(n)) + dot_rows(0, rows, 1, tile(n))
+        v = acc[1, rows, tile(n)] + dot_rows(1, rows, 2, tile(n)) + dot_rows(1, rows, -1, tile(n))
         hbuf[rows, tile(n)] = silu_mul(g, v)
 
     def hidden_later(h, n):
-        need(2, 19)
+        need(2, 18)
         rows = slice(h * 256, h * 256 + 256)
         cols = slice(n * 256, n * 256 + 256)
         xs = xbuf[1, rows, :]
@@ -373,12 +368,13 @@
         send_x(0, sign, 0)
         send_y(0, sign, 1)
         send_x(0, sign, 1)
+        send_y(0, sign, 2)
     own_partner(0)
     await_bytes(tokv, loc_sem.at[1])
     await_bytes(gains, loc_sem.at[2])
     await_bytes(mixv, loc_sem.at[6])
     tasks = dict(
-        y=y_event, x=x_event, en=early_norm, ao=ag_own, af=ag_forward, ae=ag_finish, g1=gemm1, g2=gemm2,
+        y=y_event, x=x_event, en=early_norm, ao=ag_own, af=ag_forward, ae=ag_finish, g1=gemm1,
         he=hidden_early, hl=hidden_later, d=down, c=combine, f=finish,
     )
     for name, *args in ORDER:
@@ -424,7 +420,7 @@
             pltpu.SemaphoreType.DMA((4,)),
             pltpu.SemaphoreType.DMA((4, 2, 7)),
             pltpu.SemaphoreType.DMA((4,)),
-            pltpu.SemaphoreType.DMA((20,)),
+            pltpu.SemaphoreType.DMA((19,)),
             pltpu.SemaphoreType.DMA((2,)),
             pltpu.SemaphoreType.DMA((2, 2, 3)),
             pltpu.SemaphoreType.DMA((2,)),

time: 112 us -> 106 us (0.946); the launches traced: 109 us -> 106 us
  Pallas kernels: 107 us -> 104 us
    pallas_call x1, Pallas kernels: 107 us -> 104 us  [on_device(): pl.pallas_call(kernel, out_shape=jax.ShapeDtypeStruct((128, 2048), BF), i...]
where the time goes in v3:
time: 106 us
  Pallas kernels  104 us (98%)
  local copies, waits for them, and re-layouts  1.88 us (2%)
    pallas_call x1, Pallas kernels, on_device(): pl.pallas_call(kernel, out_shape=jax.ShapeDtypeStruct((128, 2048), BF), i...  104 us

profile of v3, /device:TPU:1, one launch (start us, length us, event | category | flops | bytes accessed | tf_op | source)
XLA Modules:
  0.0 105.7 jit_solution(16921219391007991576)
XLA Ops:
  0.0 103.8 %shard_map.127 = bf16[128,2048]{1,0:T(8,128)(2,1)} custom-call(bf16[128,2048]{1,0:T(8,128)(2,1)} %tok.1, bf16[128,2048]{1,0:T(8,128)(2,1)} %mix.1, f32[1,2048]{1,0:T(1,128)} %bitcast.5, bf16[128,1280]{1,0:T(8,128)(2,1)} %eg.1, bf16[128,1280]{1,0:T(8,128)(2,1)} %ev.1, bf16[1280,128]{1,0:T(8,128)(2,1)} %ed.1, f32[1,2048]{1,0:T(1,128)} %bitcast.6, ...), custom_call_target="tpu_custom_call" | custom-call | tf_op jit(solution)/shard_map/pallas_call | solution.py:396
  103.8 1.9 %copy.15 = bf16[128,2048]{1,0:T(8,128)(2,1)} copy(bf16[128,2048]{1,0:T(8,128)(2,1)} %shard_map.127) | data formatting | bytes 1048576

commit v4 on v3

--- a/solution.py
+++ b/solution.py
@@ -14,39 +14,39 @@
 
 
 ORDER = (
-    ("en", 0), ("en", 1), ("ao", 0, 1, 0), ("ao", 0, 1, 1), ("ao", 0, 1, 2), ("ao", 0, 1, 3), ("ao", 0, 0, 0),
-    ("ao", 0, 0, 1), ("af", 0, 1, 0), ("y", 0, 0), ("x", 0, 0), ("af", 0, 1, 1), ("ao", 0, 0, 2), ("y", 0, 1),
-    ("x", 0, 1), ("ao", 0, 0, 3), ("af", 0, 0, 0), ("af", 0, 0, 1), ("y", 0, 2), ("x", 0, 2), ("ae", 0, 1),
-    ("y", 0, 3), ("x", 0, 3), ("y", 0, 4), ("x", 0, 4), ("ae", 0, 0), ("g1", 0, 1), ("g1", 0, 4), ("g1", 1, 4),
-    ("g1", 1, 2), ("y", 0, 5), ("x", 0, 5), ("g1", 0, 3), ("g1", 0, 0), ("g1", 1, 1), ("g1", 0, 2), ("g1", 1, 3),
-    ("g1", 1, 0), ("y", 0, 6), ("x", 0, 6), ("y", 1, 0), ("x", 1, 0), ("y", 1, 1), ("x", 1, 1), ("he", 1, 2),
-    ("he", 0, 4), ("he", 0, 0), ("y", 1, 2), ("he", 0, 2), ("he", 0, 1), ("x", 1, 2), ("he", 1, 4), ("y", 1, 3),
-    ("he", 1, 0), ("he", 0, 3), ("d", 0, 0, (0, 0)), ("x", 1, 3), ("d", 0, 0, (0, 1)), ("y", 1, 4), ("he", 1, 3),
-    ("he", 1, 1), ("d", 0, 1, (0, 0)), ("x", 1, 4), ("y", 1, 5), ("d", 0, 1, (0, 1)), ("x", 1, 5),
-    ("c", 0, 0, (0, 0)), ("y", 1, 6), ("d", 0, 0, (2, 0)), ("c", 0, 0, (0, 1)), ("d", 0, 1, (2, 0)), ("x", 1, 6),
-    ("d", 0, 0, (1, 0)), ("d", 0, 0, (-1, 0)), ("c", 0, 1, (0, 1)), ("d", 0, 0, (1, 1)), ("d", 0, 0, (-1, 1)),
-    ("d", 0, 0, (2, 1)), ("y", 2, 0), ("c", 0, 0, (2, 0)), ("c", 0, 1, (0, 0)), ("x", 2, 0), ("d", 0, 1, (2, 1)),
-    ("c", 0, 1, (2, 0)), ("c", 0, 0, (1, 0)), ("d", 0, 1, (-1, 1)), ("y", 2, 1), ("c", 0, 0, (-1, 0)),
-    ("d", 0, 1, (-1, 0)), ("c", 0, 0, (1, 1)), ("x", 2, 1), ("c", 0, 0, (-1, 1)), ("d", 0, 1, (1, 1)),
-    ("c", 0, 0, (2, 1)), ("d", 0, 1, (1, 0)), ("y", 2, 2), ("c", 0, 1, (2, 1)), ("x", 2, 2), ("c", 0, 1, (-1, 1)),
-    ("c", 0, 1, (-1, 0)), ("y", 2, 3), ("c", 0, 1, (1, 1)), ("f", 0, 0), ("x", 2, 3), ("ao", 1, 0, 0),
-    ("ao", 1, 0, 1), ("ao", 1, 0, 2), ("c", 0, 1, (1, 0)), ("ao", 1, 0, 3), ("y", 2, 4), ("x", 2, 4),
-    ("af", 1, 0, 0), ("y", 2, 5), ("af", 1, 0, 1), ("x", 2, 5), ("f", 0, 1), ("ao", 1, 1, 0), ("ao", 1, 1, 1),
-    ("ao", 1, 1, 2), ("y", 2, 6), ("ao", 1, 1, 3), ("x", 2, 6), ("y", 3, 0), ("ae", 1, 0), ("x", 3, 0),
-    ("y", 3, 1), ("af", 1, 1, 0), ("hl", 0, 4), ("hl", 0, 2), ("x", 3, 1), ("y", 3, 2), ("af", 1, 1, 1),
-    ("hl", 0, 1), ("hl", 0, 0), ("x", 3, 2), ("y", 3, 3), ("hl", 0, 3), ("d", 1, 0, (0, 0)), ("x", 3, 3),
-    ("d", 1, 0, (0, 1)), ("y", 3, 4), ("x", 3, 4), ("y", 3, 5), ("ae", 1, 1), ("hl", 1, 4), ("d", 1, 0, (2, 0)),
-    ("x", 3, 5), ("y", 3, 6), ("hl", 1, 2), ("c", 1, 0, (0, 1)), ("d", 1, 0, (1, 0)), ("x", 3, 6),
-    ("d", 1, 0, (-1, 0)), ("c", 1, 0, (0, 0)), ("hl", 1, 0), ("d", 1, 0, (-1, 1)), ("d", 1, 0, (1, 1)),
-    ("c", 1, 0, (2, 0)), ("hl", 1, 1), ("d", 1, 0, (2, 1)), ("c", 1, 0, (1, 0)), ("hl", 1, 3),
-    ("c", 1, 0, (-1, 0)), ("d", 1, 1, (2, 1)), ("d", 1, 1, (-1, 1)), ("d", 1, 1, (1, 0)), ("d", 1, 1, (0, 1)),
-    ("d", 1, 1, (2, 0)), ("d", 1, 1, (0, 0)), ("d", 1, 1, (1, 1)), ("d", 1, 1, (-1, 0)), ("c", 1, 1, (2, 1)),
-    ("c", 1, 0, (-1, 1)), ("c", 1, 0, (2, 1)), ("c", 1, 0, (1, 1)), ("c", 1, 1, (-1, 1)), ("c", 1, 1, (1, 0)),
-    ("c", 1, 1, (0, 1)), ("c", 1, 1, (2, 0)), ("c", 1, 1, (0, 0)), ("c", 1, 1, (1, 1)), ("c", 1, 1, (-1, 0)),
-    ("f", 1, 0), ("f", 1, 1),
+    ("en", 0), ("ao", 0, 0, 0), ("ao", 0, 0, 1), ("ao", 0, 0, 2), ("en", 1), ("ao", 0, 1, 0), ("ao", 0, 1, 1),
+    ("af", 0, 0, 0), ("ao", 0, 0, 3), ("af", 0, 0, 1), ("y", 0, 0), ("x", 0, 0), ("ao", 0, 1, 2), ("af", 0, 1, 0),
+    ("y", 0, 1), ("x", 0, 1), ("af", 0, 1, 1), ("ao", 0, 1, 3), ("y", 0, 2), ("x", 0, 2), ("ae", 0, 0),
+    ("y", 0, 3), ("x", 0, 3), ("ae", 0, 1), ("g1", 0, 1), ("y", 0, 4), ("x", 0, 4), ("g1", 1, 2), ("g1", 1, 3),
+    ("g1", 0, 2), ("g1", 0, 3), ("g1", 1, 4), ("g1", 0, 0), ("g1", 0, 4), ("g1", 1, 0), ("y", 0, 5), ("x", 0, 5),
+    ("g1", 1, 1), ("y", 0, 6), ("x", 0, 6), ("y", 1, 0), ("x", 1, 0), ("he", 1, 0), ("he", 0, 2), ("he", 1, 4),
+    ("y", 1, 1), ("x", 1, 1), ("he", 0, 0), ("he", 0, 1), ("he", 0, 4), ("he", 0, 3), ("d", 0, 0, (0, 0)),
+    ("y", 1, 2), ("d", 0, 0, (0, 1)), ("he", 1, 1), ("he", 1, 3), ("x", 1, 2), ("he", 1, 2), ("d", 0, 1, (0, 0)),
+    ("y", 1, 3), ("d", 0, 1, (0, 1)), ("x", 1, 3), ("y", 1, 4), ("d", 0, 1, (1, 0)), ("d", 0, 1, (-1, 0)),
+    ("c", 0, 0, (0, 0)), ("d", 0, 0, (-1, 0)), ("x", 1, 4), ("d", 0, 0, (1, 0)), ("y", 1, 5), ("c", 0, 0, (0, 1)),
+    ("c", 0, 1, (0, 0)), ("c", 0, 1, (0, 1)), ("x", 1, 5), ("d", 0, 0, (2, 0)), ("d", 0, 1, (2, 0)), ("y", 1, 6),
+    ("c", 0, 1, (1, 0)), ("c", 0, 1, (-1, 0)), ("d", 0, 0, (1, 1)), ("d", 0, 0, (-1, 1)), ("x", 1, 6),
+    ("d", 0, 1, (-1, 1)), ("c", 0, 0, (-1, 0)), ("d", 0, 1, (1, 1)), ("c", 0, 0, (1, 0)), ("d", 0, 1, (2, 1)),
+    ("y", 2, 0), ("d", 0, 0, (2, 1)), ("c", 0, 0, (2, 0)), ("x", 2, 0), ("c", 0, 1, (2, 0)), ("c", 0, 0, (1, 1)),
+    ("y", 2, 1), ("c", 0, 0, (-1, 1)), ("c", 0, 1, (-1, 1)), ("x", 2, 1), ("c", 0, 1, (1, 1)), ("c", 0, 1, (2, 1)),
+    ("y", 2, 2), ("c", 0, 0, (2, 1)), ("x", 2, 2), ("f", 0, 1), ("f", 0, 0), ("ao", 1, 0, 0), ("ao", 1, 0, 1),
+    ("y", 2, 3), ("ao", 1, 0, 2), ("x", 2, 3), ("ao", 1, 0, 3), ("y", 2, 4), ("x", 2, 4), ("af", 1, 0, 0),
+    ("af", 1, 0, 1), ("y", 2, 5), ("x", 2, 5), ("ao", 1, 1, 0), ("ao", 1, 1, 1), ("y", 2, 6), ("x", 2, 6),
+    ("ao", 1, 1, 2), ("ae", 1, 0), ("gl", 0, 4), ("y", 3, 0), ("gl", 0, 0), ("gl", 0, 2), ("ao", 1, 1, 3),
+    ("gl", 0, 1), ("af", 1, 1, 0), ("x", 3, 0), ("hl", 0, 1), ("y", 3, 1), ("hl", 0, 2), ("hl", 0, 4),
+    ("gl", 0, 3), ("x", 3, 1), ("af", 1, 1, 1), ("hl", 0, 3), ("hl", 0, 0), ("y", 3, 2), ("d", 1, 0, (0, 0)),
+    ("d", 1, 0, (0, 1)), ("x", 3, 2), ("y", 3, 3), ("x", 3, 3), ("d", 1, 0, (1, 0)), ("y", 3, 4),
+    ("d", 1, 0, (-1, 0)), ("ae", 1, 1), ("gl", 1, 4), ("x", 3, 4), ("gl", 1, 0), ("c", 1, 0, (0, 0)), ("y", 3, 5),
+    ("hl", 1, 0), ("gl", 1, 1), ("hl", 1, 1), ("x", 3, 5), ("c", 1, 0, (0, 1)), ("gl", 1, 2), ("c", 1, 0, (1, 0)),
+    ("d", 1, 0, (2, 0)), ("y", 3, 6), ("hl", 1, 2), ("c", 1, 0, (-1, 0)), ("x", 3, 6), ("d", 1, 0, (-1, 1)),
+    ("d", 1, 0, (1, 1)), ("hl", 1, 4), ("gl", 1, 3), ("d", 1, 0, (2, 1)), ("hl", 1, 3), ("d", 1, 1, (2, 1)),
+    ("d", 1, 1, (2, 0)), ("c", 1, 0, (2, 0)), ("d", 1, 1, (-1, 1)), ("d", 1, 1, (0, 0)), ("d", 1, 1, (1, 0)),
+    ("c", 1, 0, (-1, 1)), ("d", 1, 1, (0, 1)), ("d", 1, 1, (-1, 0)), ("d", 1, 1, (1, 1)), ("c", 1, 0, (2, 1)),
+    ("c", 1, 0, (1, 1)), ("c", 1, 1, (2, 1)), ("c", 1, 1, (2, 0)), ("c", 1, 1, (-1, 1)), ("c", 1, 1, (0, 0)),
+    ("c", 1, 1, (1, 0)), ("c", 1, 1, (0, 1)), ("c", 1, 1, (-1, 0)), ("c", 1, 1, (1, 1)), ("f", 1, 0), ("f", 1, 1),
 )
-OWN_Y_AT = 3
-OWN_X_AT = 4
+OWN_Y_AT = 4
+OWN_X_AT = 5
 
 
 def kernel(
@@ -113,28 +113,26 @@
 
     def y_recv_content(sign, k):
         t = tee(sign)
-        return [(-sign, 0, t, 0), (-sign, 0, t, 1), (-sign, 0, 1 - t, 0), (2, 0, t, 0), (2, 0, t, 1),
-                (-sign, 0, 1 - t, 1), (-sign, 1, 1 - t, 1)][k]
+        return [(-sign, 0, t, 0), (-sign, 0, t, 1), (-sign, 0, 1 - t, 0), (-sign, 0, 1 - t, 1), (2, 0, t, 0),
+                (2, 0, t, 1), (2, 1, t, 1)][k]
 
     def y_send_content(sign, k):
         t = tee(sign)
-        return [(0, 0, t, 0), (0, 0, t, 1), (0, 0, 1 - t, 0), (-sign, 0, t, 0), (-sign, 0, t, 1),
-                (0, 0, 1 - t, 1), (0, 1, 1 - t, 1)][k]
+        return [(0, 0, t, 0), (0, 0, t, 1), (0, 0, 1 - t, 0), (0, 0, 1 - t, 1), (-sign, 0, t, 0),
+                (-sign, 0, t, 1), (-sign, 1, t, 1)][k]
 
     def x_content(sign, k, dp):
         t = tee(sign)
         return [(0, dp, t, 0), (0, dp, t, 1), (-sign, dp, t, 0), (-sign, dp, t, 1), (sign, dp, t, 0),
-                (2, dp, t, 0), (2, dp, t, 1)][k]
+                (sign, dp, t, 1), (2, dp, t, 0)][k]
 
     have = set()
     partner_have = set()
 
     def group_of(r, content):
         dy, dp, st, s = content
-        if r == 2:
-            return 18
-        if r == 0:
-            return 0 if dy in (0, -1 if st == 0 else 1) else 1
+        if r % 2 == 0:
+            return r * 9 + (0 if dy in (0, -1 if st == 0 else 1) else 1)
         return 2 + (r // 2) * 8 + (dy % 4) * 2 + dp
 
     def send_y(r, sign, k):
@@ -165,7 +163,7 @@
     def own_y(r):
         wait_local(r)
         for sign in (1, -1):
-            for k in (0, 1, 2):
+            for k in (0, 1, 2, 3):
                 send_y(r, sign, k)
 
     def own_x(r):
@@ -183,19 +181,12 @@
         for sign in (1, -1):
             have.add((r, y_recv_content(sign, j)))
         for sign in (1, -1):
-            if j == 0:
-                send_x(r, sign, 2)
-                send_y(r, sign, 3)
-            elif j == 1:
-                send_x(r, sign, 3)
-                send_y(r, sign, 4)
-                send_y(r, sign, 5)
-            elif j == 2:
-                send_x(r, -sign, 4)
-            elif j == 3:
-                send_x(r, sign, 5)
-            elif j == 4:
-                send_x(r, sign, 6)
+            if j in (2, 3):
+                send_x(r, -sign, j + 2)
+            elif j < 5:
+                send_x(r, sign, j + 2)
+            if j < 2:
+                send_y(r, sign, j + 4)
         if r < 3 and j == OWN_Y_AT:
             own_y(r + 1)
         if r < 3 and j == OWN_X_AT:
@@ -210,7 +201,7 @@
         for sign in (1, -1):
             have.add((r, x_content(sign, j, 1)))
         for sign in (1, -1):
-            if j == 1:
+            if j == 3:
                 send_y(r, sign, 6)
             send_partner(r, x_content(sign, j, 1))
 
@@ -269,10 +260,10 @@
 
         lax.fori_loop(0, 4, body, 0)
 
-    def dot_rows(st, rows, dy, cols):
+    def dot_rows(st, rows, dy, cols, layer=0):
         base = pl.multiple_of(mod4(y + dy) * 512, 512)
         w = gbuf if st == 0 else vbuf
-        return jnp.dot(xbuf[0, rows, pl.ds(base, 512)], w[0, pl.ds(base, 512), cols], preferred_element_type=F32)
+        return jnp.dot(xbuf[layer, rows, pl.ds(base, 512)], w[layer, pl.ds(base, 512), cols], preferred_element_type=F32)
 
     whole = slice(0, 512)
 
@@ -286,23 +277,26 @@
     def silu_mul(g, v):
         return (g * (1.0 / (1.0 + jnp.exp(-g))) * v).astype(BF)
 
-    def hidden_early(h, n):
-        need(0, 1)
-        rows = slice(h * 256, h * 256 + 256)
-        g = acc[0, rows, tile(n)] + dot_rows(0, rows, 2, tile(n)) + dot_rows(0, rows, 1, tile(n))
-        v = acc[1, rows, tile(n)] + dot_rows(1, rows, 2, tile(n)) + dot_rows(1, rows, -1, tile(n))
-        hbuf[rows, tile(n)] = silu_mul(g, v)
-
-    def hidden_later(h, n):
+    def gemm1_later(h, n):
         need(2, 18)
         rows = slice(h * 256, h * 256 + 256)
-        cols = slice(n * 256, n * 256 + 256)
-        xs = xbuf[1, rows, :]
-        g = jnp.dot(xs, gbuf[1, :, cols], preferred_element_type=F32)
-        v = jnp.dot(xs, vbuf[1, :, cols], preferred_element_type=F32)
-        hbuf[rows, cols] = silu_mul(g, v)
-
-    chunks = ((0, 0), (0, 1), (2, 0), (-1, 0), (1, 0), (2, 1), (-1, 1), (1, 1))
+        for st in (0, 1):
+            acc[st, rows, tile(n)] = dot_rows(st, rows, 0, tile(n), 1) + dot_rows(st, rows, -1 if st == 0 else 1, tile(n), 1)
+
+    def hidden(layer, h, n):
+        need(2 * layer, 18 * layer + 1)
+        rows = slice(h * 256, h * 256 + 256)
+        g = acc[0, rows, tile(n)] + dot_rows(0, rows, 2, tile(n), layer) + dot_rows(0, rows, 1, tile(n), layer)
+        v = acc[1, rows, tile(n)] + dot_rows(1, rows, 2, tile(n), layer) + dot_rows(1, rows, -1, tile(n), layer)
+        hbuf[rows, tile(n)] = silu_mul(g, v)
+
+    def hidden_early(h, n):
+        hidden(0, h, n)
+
+    def hidden_later(h, n):
+        hidden(1, h, n)
+
+    chunks = ((0, 0), (0, 1), (-1, 0), (1, 0), (2, 0), (-1, 1), (1, 1), (2, 1))
 
     def down(layer, h, chunk):
         r = 2 * layer + 1
@@ -369,12 +363,13 @@
         send_y(0, sign, 1)
         send_x(0, sign, 1)
         send_y(0, sign, 2)
+        send_y(0, sign, 3)
     own_partner(0)
     await_bytes(tokv, loc_sem.at[1])
     await_bytes(gains, loc_sem.at[2])
     await_bytes(mixv, loc_sem.at[6])
     tasks = dict(
-        y=y_event, x=x_event, en=early_norm, ao=ag_own, af=ag_forward, ae=ag_finish, g1=gemm1,
+        y=y_event, x=x_event, en=early_norm, ao=ag_own, af=ag_forward, ae=ag_finish, g1=gemm1, gl=gemm1_later,
         he=hidden_early, hl=hidden_later, d=down, c=combine, f=finish,
     )
     for name, *args in ORDER:
@@ -420,7 +415,7 @@
             pltpu.SemaphoreType.DMA((4,)),
             pltpu.SemaphoreType.DMA((4, 2, 7)),
             pltpu.SemaphoreType.DMA((4,)),
-            pltpu.SemaphoreType.DMA((19,)),
+            pltpu.SemaphoreType.DMA((20,)),
             pltpu.SemaphoreType.DMA((2,)),
             pltpu.SemaphoreType.DMA((2, 2, 3)),
             pltpu.SemaphoreType.DMA((2,)),

time: 106 us -> 108 us (1.019)
    pallas_call x1, Pallas kernels: 104 us -> 105 us  [on_device(): pl.pallas_call(kernel, out_shape=jax.ShapeDtypeStruct((128, 2048), BF), i...]
where the time goes in v4:
time: 108 us; the launch traced here: 107 us
  Pallas kernels  105 us (97%)
  local copies, waits for them, and re-layouts  1.88 us (2%)
    pallas_call x1, Pallas kernels, on_device(): pl.pallas_call(kernel, out_shape=jax.ShapeDtypeStruct((128, 2048), BF), i...  105 us

profile of v4, /device:TPU:1, one launch (start us, length us, event | category | flops | bytes accessed | tf_op | source)
XLA Modules:
  0.0 107.0 jit_solution(16985436625737878619)
XLA Ops:
  0.0 105.1 %shard_map.127 = bf16[128,2048]{1,0:T(8,128)(2,1)} custom-call(bf16[128,2048]{1,0:T(8,128)(2,1)} %tok.1, bf16[128,2048]{1,0:T(8,128)(2,1)} %mix.1, f32[1,2048]{1,0:T(1,128)} %bitcast.5, bf16[128,1280]{1,0:T(8,128)(2,1)} %eg.1, bf16[128,1280]{1,0:T(8,128)(2,1)} %ev.1, bf16[1280,128]{1,0:T(8,128)(2,1)} %ed.1, f32[1,2048]{1,0:T(1,128)} %bitcast.6, ...), custom_call_target="tpu_custom_call" | custom-call | tf_op jit(solution)/shard_map/pallas_call | solution.py:391
  105.1 1.9 %copy.15 = bf16[128,2048]{1,0:T(8,128)(2,1)} copy(bf16[128,2048]{1,0:T(8,128)(2,1)} %shard_map.127) | data formatting | bytes 1048576

commit v5 on v4

v5 whole, which is shorter than its diff:
```python
import functools

import jax
import jax.numpy as jnp
from jax import lax
from jax.experimental import pallas as pl
from jax.experimental.pallas import tpu as pltpu
from jax.sharding import PartitionSpec as P

MESH = pl.DeviceIdType.MESH
EPS = 1e-06
BF = jnp.bfloat16
F32 = jnp.float32


ORDER = (
    ("en", 0), ("en", 1), ("ao", 0, 1, 0), ("ao", 0, 0, 0), ("ao", 0, 0, 1), ("ao", 0, 0, 2), ("ao", 0, 0, 3),
    ("ao", 0, 1, 1), ("af", 0, 1, 0), ("y", 0, 0), ("af", 0, 0, 0), ("af", 0, 0, 1), ("x", 0, 1), ("y", 0, 1),
    ("ao", 0, 1, 2), ("ao", 0, 1, 3), ("af", 0, 1, 1), ("y", 0, 2), ("ae", 0, 0), ("x", 0, 3), ("y", 0, 3),
    ("y", 0, 4), ("ae", 0, 1), ("g1", 0), ("g1", 1), ("x", 0, 5), ("y", 0, 5), ("g2", 1), ("y", 0, 6), ("x", 0, 6),
    ("g2", 0), ("y", 1, 0), ("x", 1, 1), ("he", 1), ("y", 1, 1), ("he", 0), ("y", 1, 2), ("d", 0, 0, 0),
    ("d", 0, 0, 1), ("d", 0, 1, 1), ("y", 1, 3), ("d", 0, 1, 0), ("d", 0, 1, 2), ("x", 1, 3), ("y", 1, 4),
    ("d", 0, 0, 2), ("c", 0, 0, (0, 0)), ("y", 1, 5), ("c", 0, 0, (0, 1)), ("c", 0, 1, (0, 1)), ("d", 0, 0, 3),
    ("c", 0, 1, (0, 0)), ("x", 1, 5), ("d", 0, 1, 3), ("c", 0, 1, (-1, 0)), ("c", 0, 1, (1, 0)), ("y", 1, 6),
    ("c", 0, 0, (-1, 0)), ("x", 1, 6), ("d", 0, 0, 4), ("c", 0, 0, (1, 0)), ("d", 0, 0, 5), ("d", 0, 1, 4),
    ("c", 0, 0, (2, 0)), ("y", 2, 0), ("c", 0, 1, (2, 0)), ("d", 0, 1, 5), ("c", 0, 0, (-1, 1)),
    ("c", 0, 0, (1, 1)), ("y", 2, 1), ("c", 0, 0, (2, 1)), ("x", 2, 1), ("c", 0, 1, (-1, 1)), ("c", 0, 1, (1, 1)),
    ("c", 0, 1, (2, 1)), ("y", 2, 2), ("f", 0, 0), ("ao", 1, 0, 0), ("ao", 1, 0, 1), ("ao", 1, 0, 2),
    ("ao", 1, 0, 3), ("f", 0, 1), ("y", 2, 3), ("x", 2, 3), ("ao", 1, 1, 0), ("af", 1, 0, 0), ("y", 2, 4),
    ("af", 1, 0, 1), ("ao", 1, 1, 1), ("y", 2, 5), ("x", 2, 5), ("ao", 1, 1, 2), ("af", 1, 1, 0), ("ao", 1, 1, 3),
    ("y", 2, 6), ("ae", 1, 0), ("gl", 0), ("x", 2, 6), ("y", 3, 0), ("af", 1, 1, 1), ("y", 3, 1), ("x", 3, 1),
    ("hl", 0), ("d", 1, 0, 0), ("y", 3, 2), ("d", 1, 0, 1), ("y", 3, 3), ("ae", 1, 1), ("gl", 1), ("d", 1, 0, 2),
    ("x", 3, 3), ("y", 3, 4), ("c", 1, 0, (0, 0)), ("hl", 1), ("d", 1, 1, 0), ("d", 1, 1, 1), ("d", 1, 1, 2),
    ("c", 1, 0, (0, 1)), ("y", 3, 5), ("x", 3, 5), ("c", 1, 0, (-1, 0)), ("c", 1, 0, (1, 0)), ("d", 1, 1, 3),
    ("d", 1, 0, 3), ("d", 1, 0, 4), ("c", 1, 1, (0, 0)), ("x", 3, 6), ("y", 3, 6), ("c", 1, 1, (0, 1)),
    ("c", 1, 1, (-1, 0)), ("c", 1, 1, (1, 0)), ("d", 1, 0, 5), ("d", 1, 1, 5), ("c", 1, 1, (2, 0)), ("d", 1, 1, 4),
    ("c", 1, 0, (2, 0)), ("c", 1, 0, (-1, 1)), ("c", 1, 0, (1, 1)), ("c", 1, 0, (2, 1)), ("c", 1, 1, (2, 1)),
    ("c", 1, 1, (-1, 1)), ("c", 1, 1, (1, 1)), ("f", 1, 0), ("f", 1, 1),
)
OWN_Y_AT = 4
OWN_X_AT = 4


def kernel(
    tok, mix, en, eg, ev, ed, ep, mg, ln, lg, lv, ld, lp,
    out,
    gbuf, vbuf, dbuf, xbuf, acc, hbuf, tokv, mixv, mixed, gains,
    rs1, rr1, rs2, rr2, keep, br, pbuf,
    loc_sem, w_send, w_recv, p_send, p_recv, ag_send, ag_recv, rs_send, rs1_recv, rs2_recv,
):
    rep = lax.axis_index("rep")
    fs = lax.axis_index("fs")
    z = lax.axis_index("tp")
    c = lax.rem(fs, 2)
    xl = lax.rem(fs // 2, 2)
    y = fs // 4
    x = rep * 2 + xl

    def mod4(v):
        return lax.rem(v + 8, 4)

    def dev(dx=0, dy=0, dz=0, dc=0):
        nx = mod4(x + dx)
        ny = mod4(y + dy)
        nc = c if dc == 0 else 1 - c
        return (nx // 2, (ny * 2 + lax.rem(nx, 2)) * 2 + nc, mod4(z + dz))

    y_dev = {1: dev(dy=1), -1: dev(dy=-1)}
    x_dev = {1: dev(dx=1), -1: dev(dx=-1)}
    z_dev = {1: dev(dz=1), -1: dev(dz=-1)}
    partner = dev(dc=1)
    everyone = [y_dev[1], y_dev[-1], x_dev[1], x_dev[-1], z_dev[1], z_dev[-1], partner]
    zp, zm, zo = mod4(z + 1), mod4(z - 1), mod4(z + 2)

    def blk_of(dy, dp):
        return mod4(y + dy) * 2 + (xl if dp == 0 else 1 - xl)

    blocks = {(dy, dp): blk_of(dy, dp) for dy in (0, 1, -1, 2) for dp in (0, 1)}

    def unit(r, content, core):
        dy, dp, st, s = content
        blk = blocks[(dy, dp)]
        layer = r // 2
        if r % 2 == 0:
            buf = gbuf if st == 0 else vbuf
            row = pl.multiple_of(blk * 256 + core * 128 + s * 64, 64)
            return buf.at[layer, pl.ds(row, 64), :]
        return dbuf.at[layer, blk, core, pl.ds(st * 640 + s * 320, 320), :]

    def unit_id(content):
        dy, dp, st, s = content
        return (((dy % 4) * 2 + dp) * 2 + st) * 2 + s

    def send(src, dst, send_sem, recv_sem, target):
        pltpu.make_async_remote_copy(src, dst, send_sem, recv_sem, device_id=target, device_id_type=MESH).start()

    def await_bytes(ref, sem):
        pltpu.make_async_copy(ref, ref, sem).wait()

    def units(r, n):
        return gbuf.at[0, pl.ds(0, n * (64 if r % 2 == 0 else 32)), :]

    def tee(sign):
        return 0 if sign > 0 else 1

    def y_recv_content(sign, k):
        t = tee(sign)
        return [(-sign, 0, t, 0), (-sign, 0, t, 1), (-sign, 0, 1 - t, 0), (-sign, 0, 1 - t, 1), (2, 0, t, 0),
                (2, 0, t, 1), (2, 1, t, 1)][k]

    def y_send_content(sign, k):
        t = tee(sign)
        return [(0, 0, t, 0), (0, 0, t, 1), (0, 0, 1 - t, 0), (0, 0, 1 - t, 1), (-sign, 0, t, 0),
                (-sign, 0, t, 1), (-sign, 1, t, 1)][k]

    def x_content(sign, k, dp):
        t = tee(sign)
        return [(0, dp, t, 0), (0, dp, t, 1), (-sign, dp, t, 0), (-sign, dp, t, 1), (sign, dp, t, 0),
                (sign, dp, t, 1), (2, dp, t, 0)][k]

    have = set()
    partner_have = set()

    def group_of(r, content):
        dy, dp, st, s = content
        if r % 2 == 0:
            return (0 if r == 0 else 19) + (0 if dy in (0, -1 if st == 0 else 1) else 2 if dy == 2 else 1)
        return 3 + (r // 2) * 8 + (dy % 4) * 2 + dp

    def send_y(r, sign, k):
        content = y_send_content(sign, k)
        assert (r, content) in have
        ref = unit(r, content, c)
        send(ref, ref, w_send.at[r], w_recv.at[r, k], y_dev[sign])

    def send_x(r, sign, k):
        content = x_content(sign, k, 0)
        assert (r, content) in have
        ref = unit(r, content, c)
        send(ref, ref, w_send.at[r], w_recv.at[r, 7 + k // 2], x_dev[sign])

    def send_partner(r, content):
        ref = unit(r, content, c)
        send(ref, ref, p_send.at[r], p_recv.at[group_of(r, content)], partner)

    every = [(dy, dp, st, s) for dy in (0, 1, -1, 2) for dp in (0, 1) for st in (0, 1) for s in (0, 1)]

    def need(r, group):
        members = [content for content in every if group_of(r, content) == group]
        assert all((r, content) in have for content in members), (r, group)
        if group not in partner_have:
            partner_have.add(group)
            await_bytes(units(r, len(members)), p_recv.at[group])

    def own_y(r):
        wait_local(r)
        for sign in (1, -1):
            for k in (0, 1, 2, 3):
                send_y(r, sign, k)

    def own_x(r):
        for sign in (1, -1):
            send_x(r, sign, 0)
            send_x(r, sign, 1)

    def own_partner(r):
        for st in (0, 1):
            for s in (0, 1):
                send_partner(r, (0, 0, st, s))

    def y_event(r, j):
        await_bytes(units(r, 2), w_recv.at[r, j])
        for sign in (1, -1):
            have.add((r, y_recv_content(sign, j)))
        for sign in (1, -1):
            if j in (2, 3):
                send_x(r, -sign, j + 2)
            elif j < 5:
                send_x(r, sign, j + 2)
            if j < 2:
                send_y(r, sign, j + 4)
        if r < 3 and j == OWN_Y_AT:
            own_y(r + 1)
        if r < 3 and j == OWN_X_AT:
            own_x(r + 1)
        for sign in (1, -1):
            send_partner(r, y_recv_content(sign, j))
        if r < 3 and j == OWN_Y_AT:
            own_partner(r + 1)

    def x_event(r, j):
        ks = (6,) if j == 6 else (j - 1, j)
        await_bytes(units(r, 2 * len(ks)), w_recv.at[r, 7 + ks[0] // 2])
        for sign in (1, -1):
            for k in ks:
                have.add((r, x_content(sign, k, 1)))
            if j == 3:
                send_y(r, sign, 6)
        for k in ks:
            for sign in (1, -1):
                send_partner(r, x_content(sign, k, 1))

    own = pl.multiple_of(blocks[(0, 0)] * 256 + c * 128, 128)
    weights = {
        0: [(eg, gbuf.at[0, pl.ds(own, 128), :]), (ev, vbuf.at[0, pl.ds(own, 128), :])],
        1: [(ed, dbuf.at[0, blocks[(0, 0)], c])],
        2: [(lg, gbuf.at[1, pl.ds(own, 128), :]), (lv, vbuf.at[1, pl.ds(own, 128), :])],
        3: [(ld, dbuf.at[1, blocks[(0, 0)], c])],
    }
    norms = [(g, gains.at[i]) for i, g in enumerate((en, ep, mg, ln, lp))]
    for i, pairs in enumerate((weights[0], [(tok, tokv)], norms, weights[1], weights[2], weights[3], [(mix, mixv)])):
        for src, dst in pairs:
            pltpu.make_async_copy(src, dst, loc_sem.at[i]).start()

    def wait_local(r):
        await_bytes(units(r, 4), loc_sem.at[(0, 3, 4, 5)[r]])
        for st in (0, 1):
            for s in (0, 1):
                have.add((r, (0, 0, st, s)))

    barrier = pltpu.get_barrier_semaphore()
    for other in everyone:
        pl.semaphore_signal(barrier, inc=1, device_id=other, device_id_type=MESH)
    pl.semaphore_wait(barrier, len(everyone))

    def x_rows(layer, h, zz, u, n=16):
        row = pl.multiple_of(h * 256 + zz * 64 + u * 16, 16)
        return xbuf.at[layer, pl.ds(row, n), :]

    def ag_own(layer, h, u):
        for sign in (1, -1):
            v = u if sign > 0 else (u + 2) % 4
            ref = x_rows(layer, h, z, v)
            send(ref, ref, ag_send.at[layer], ag_recv.at[h, min(u, 2)], z_dev[sign])

    def ag_forward(layer, h, u):
        await_bytes(xbuf.at[0, pl.ds(0, 32), :], ag_recv.at[h, u])
        for sign in (1, -1):
            v = u if sign > 0 else u + 2
            ref = x_rows(layer, h, zm if sign > 0 else zp, v)
            send(ref, ref, ag_send.at[layer], ag_recv.at[h, 2], z_dev[sign])

    def ag_finish(layer, h):
        await_bytes(xbuf.at[0, pl.ds(0, 128), :], ag_recv.at[h, 2])

    def rms(v, gain):
        return v * lax.rsqrt(jnp.mean(v * v, axis=-1, keepdims=True) + EPS) * gain

    def early_norm(h):
        for i in range(4):
            v = rms(tokv[h * 64 + i * 16 : h * 64 + i * 16 + 16, :].astype(F32), gains[0])
            x_rows(0, h, z, i)[...] = v.astype(BF)

    def dot_rows(st, rows, dy, cols, layer=0):
        base = pl.multiple_of(mod4(y + dy) * 512, 512)
        w = gbuf if st == 0 else vbuf
        return jnp.dot(xbuf[layer, rows, pl.ds(base, 512)], w[layer, pl.ds(base, 512), cols], preferred_element_type=F32)

    whole = slice(0, 512)

    def tile(n):
        return slice(n * 256, n * 256 + 256)

    def gemm1(st):
        need(0, 0)
        for n in range(5):
            acc[st, :, tile(n)] = dot_rows(st, whole, 0, tile(n)) + dot_rows(st, whole, -1 if st == 0 else 1, tile(n))

    def silu_mul(g, v):
        return (g * (1.0 / (1.0 + jnp.exp(-g))) * v).astype(BF)

    def gemm2(st):
        need(0, 1)
        for n in range(5):
            acc[st, :, tile(n)] += dot_rows(st, whole, 1 if st == 0 else -1, tile(n))

    def gemm1_later(h):
        need(2, 19)
        need(2, 20)
        rows = slice(h * 256, h * 256 + 256)
        for n in range(5):
            for st in (0, 1):
                parts = [dot_rows(st, rows, dy, tile(n), 1) for dy in (0, -1, 1)]
                acc[st, rows, tile(n)] = parts[0] + parts[1] + parts[2]

    def hidden(layer, h):
        need(2 * layer, 19 * layer + 2)
        rows = slice(h * 256, h * 256 + 256)
        for n in range(5):
            g = acc[0, rows, tile(n)] + dot_rows(0, rows, 2, tile(n), layer)
            v = acc[1, rows, tile(n)] + dot_rows(1, rows, 2, tile(n), layer)
            hbuf[rows, tile(n)] = silu_mul(g, v)

    def hidden_early(h):
        hidden(0, h)

    def hidden_later(h):
        hidden(1, h)

    chunks = ((0, 0), (0, 1), (-1, 0), (1, 0), (2, 0), (-1, 1), (1, 1), (2, 1))

    groups = (((0, 0),), ((0, 1),), ((-1, 0), (1, 0)), ((2, 0),), ((-1, 1), (1, 1)), ((2, 1),))

    def down(layer, h, i):
        r = 2 * layer + 1

        def rows(zz, half):
            return pl.ds(pl.multiple_of(zz * 64 + half * 32, 32), 32)

        for dy, dp in groups[i]:
            need(r, group_of(r, (dy, dp, 0, 0)))
        for k, chunk in enumerate(groups[i]):
            blk = blocks[chunk]
            w = jnp.concatenate([dbuf[layer, blk, 0], dbuf[layer, blk, 1]], axis=1)
            pbuf[k] = jnp.dot(hbuf[h * 256 : h * 256 + 256, :], w, preferred_element_type=F32)
        for k, chunk in enumerate(groups[i]):
            j = chunks.index(chunk)
            rs1[layer, h, j, 0, 0:32, :] = pbuf[k, rows(zo, 0), :].astype(BF)
            rs1[layer, h, j, 0, 32:64, :] = pbuf[k, rows(zp, 1), :].astype(BF)
            rs1[layer, h, j, 1, 0:32, :] = pbuf[k, rows(zm, 0), :].astype(BF)
            rs1[layer, h, j, 1, 32:64, :] = pbuf[k, rows(zo, 1), :].astype(BF)
            keep[h, j, 0] = pbuf[k, rows(zp, 0), :]
            keep[h, j, 1] = pbuf[k, rows(zm, 1), :]
            cols = pl.ds(pl.multiple_of(blocks[chunk] * 256, 256), 256)
            br[h * 64 : h * 64 + 64, cols] = pbuf[k, pl.ds(pl.multiple_of(z * 64, 64), 64), :]
        for chunk in groups[i]:
            j = chunks.index(chunk)
            for sign in (1, -1):
                lane = tee(sign)
                send(rs1.at[layer, h, j, lane], rr1.at[layer, h, j, lane], rs_send.at[0], rs1_recv.at[h, j], z_dev[sign])

    def combine(layer, h, chunk):
        j = chunks.index(chunk)
        await_bytes(rr1.at[layer, h, j], rs1_recv.at[h, j])
        for sign in (1, -1):
            lane = tee(sign)
            half = slice(0, 32) if sign > 0 else slice(32, 64)
            rs2[layer, h, j, lane] = (rr1[layer, h, j, lane, half, :].astype(F32) + keep[h, j, lane]).astype(BF)
        for sign in (1, -1):
            lane = tee(sign)
            send(rs2.at[layer, h, j, lane], rr2.at[layer, h, j, lane], rs_send.at[1], rs2_recv.at[h], z_dev[sign])
        cols = pl.ds(pl.multiple_of(blocks[chunk] * 256, 256), 256)
        br[h * 64 : h * 64 + 32, cols] += rr1[layer, h, j, 1, 0:32, :].astype(F32)
        br[h * 64 + 32 : h * 64 + 64, cols] += rr1[layer, h, j, 0, 32:64, :].astype(F32)

    def finish(layer, h):
        await_bytes(rr2.at[layer, h], rs2_recv.at[h])
        for j, chunk in enumerate(chunks):
            cols = pl.ds(pl.multiple_of(blocks[chunk] * 256, 256), 256)
            br[h * 64 : h * 64 + 32, cols] += rr2[layer, h, j, 0].astype(F32)
            br[h * 64 + 32 : h * 64 + 64, cols] += rr2[layer, h, j, 1].astype(F32)
        for i in range(4):
            rows = slice(h * 64 + i * 16, h * 64 + i * 16 + 16)
            branch = br[rows, :]
            if layer == 0:
                m = tokv[rows, :].astype(F32) + 0.5 * rms(branch, gains[1]) + rms(mixv[rows, :].astype(F32), gains[2])
                m = m.astype(BF)
                mixed[rows, :] = m
                x_rows(1, h, z, i)[...] = rms(m.astype(F32), gains[3]).astype(BF)
            else:
                out[rows, :] = (mixed[rows, :].astype(F32) + 0.5 * rms(branch, gains[4])).astype(BF)

    wait_local(0)
    for sign in (1, -1):
        send_y(0, sign, 0)
        send_x(0, sign, 0)
        send_y(0, sign, 1)
        send_x(0, sign, 1)
        send_y(0, sign, 2)
        send_y(0, sign, 3)
    own_partner(0)
    await_bytes(tokv, loc_sem.at[1])
    await_bytes(gains, loc_sem.at[2])
    await_bytes(mixv, loc_sem.at[6])
    tasks = dict(
        y=y_event, x=x_event, en=early_norm, ao=ag_own, af=ag_forward, ae=ag_finish, g1=gemm1, g2=gemm2, gl=gemm1_later,
        he=hidden_early, hl=hidden_later, d=down, c=combine, f=finish,
    )
    for name, *args in ORDER:
        fn = tasks[name]
        fn(*args)

    for r in range(4):
        await_bytes(units(r, 28), w_send.at[r])
        await_bytes(units(r, 32), p_send.at[r])
    for layer in (0, 1):
        await_bytes(xbuf.at[0, pl.ds(0, 384), :], ag_send.at[layer])
    await_bytes(rs1, rs_send.at[0])
    await_bytes(rs2, rs_send.at[1])


def on_device(tokens, mixer_output, en, eg, ev, ed, ep, mg, ln, lg, lv, ld, lp):
    gains = [g.reshape(1, 2048) for g in (en, ep, mg, ln, lp)]
    en, ep, mg, ln, lp = gains
    return pl.pallas_call(
        kernel,
        out_shape=jax.ShapeDtypeStruct((128, 2048), BF),
        in_specs=[pl.BlockSpec(memory_space=pl.ANY)] * 13,
        out_specs=pl.BlockSpec(memory_space=pltpu.VMEM),
        scratch_shapes=[
            pltpu.VMEM((2, 2048, 1280), BF),
            pltpu.VMEM((2, 2048, 1280), BF),
            pltpu.VMEM((2, 8, 2, 1280, 128), BF),
            pltpu.VMEM((2, 512, 2048), BF),
            pltpu.VMEM((2, 512, 1280), F32),
            pltpu.VMEM((512, 1280), BF),
            pltpu.VMEM((128, 2048), BF),
            pltpu.VMEM((128, 2048), BF),
            pltpu.VMEM((128, 2048), BF),
            pltpu.VMEM((5, 1, 2048), F32),
            pltpu.VMEM((2, 2, 8, 2, 64, 256), BF),
            pltpu.VMEM((2, 2, 8, 2, 64, 256), BF),
            pltpu.VMEM((2, 2, 8, 2, 32, 256), BF),
            pltpu.VMEM((2, 2, 8, 2, 32, 256), BF),
            pltpu.VMEM((2, 8, 2, 32, 256), F32),
            pltpu.VMEM((128, 2048), F32),
            pltpu.VMEM((2, 256, 256), F32),
            pltpu.SemaphoreType.DMA((7,)),
            pltpu.SemaphoreType.DMA((4,)),
            pltpu.SemaphoreType.DMA((4, 11)),
            pltpu.SemaphoreType.DMA((4,)),
            pltpu.SemaphoreType.DMA((22,)),
            pltpu.SemaphoreType.DMA((2,)),
            pltpu.SemaphoreType.DMA((2, 3)),
            pltpu.SemaphoreType.DMA((2,)),
            pltpu.SemaphoreType.DMA((2, 8)),
            pltpu.SemaphoreType.DMA((2,)),
        ],
        compiler_params=pltpu.CompilerParams(
            collective_id=0, has_side_effects=True, vmem_limit_bytes=67_000_000
        ),
    )(tokens, mixer_output, en, eg, ev, ed, ep, mg, ln, lg, lv, ld, lp)


def solution(mesh):
    placed = (
        P(("rep", "fs", "tp"), None),
        P(("rep", "fs", "tp"), None),
        P(),
        P("fs", "tp"),
        P("fs", "tp"),
        P("tp", "fs"),
        P(),
        P(),
        P(),
        P("fs", "tp"),
        P("fs", "tp"),
        P("tp", "fs"),
        P(),
    )
    return jax.shard_map(
        on_device,
        mesh=mesh,
        in_specs=placed,
        out_specs=P(("rep", "fs", "tp"), None),
        check_vma=False,
    )
```

time: 108 us -> 105 us (0.972)
  Pallas kernels: 105 us -> 102 us
    pallas_call x1, Pallas kernels: 105 us -> 102 us  [on_device(): pl.pallas_call(kernel, out_shape=jax.ShapeDtypeStruct((128, 2048), BF), i...]
where the time goes in v5:
time: 105 us; the launch traced here: 104 us
  Pallas kernels  102 us (97%)
  local copies, waits for them, and re-layouts  1.88 us (2%)
    pallas_call x1, Pallas kernels, on_device(): pl.pallas_call(kernel, out_shape=jax.ShapeDtypeStruct((128, 2048), BF), i...  102 us

profile of v5, /device:TPU:1, one launch (start us, length us, event | category | flops | bytes accessed | tf_op | source)
XLA Modules:
  0.0 104.0 jit_solution(6048380976415220210)
XLA Ops:
  0.0 102.1 %shard_map.127 = bf16[128,2048]{1,0:T(8,128)(2,1)} custom-call(bf16[128,2048]{1,0:T(8,128)(2,1)} %tok.1, bf16[128,2048]{1,0:T(8,128)(2,1)} %mix.1, f32[1,2048]{1,0:T(1,128)} %bitcast.5, bf16[128,1280]{1,0:T(8,128)(2,1)} %eg.1, bf16[128,1280]{1,0:T(8,128)(2,1)} %ev.1, bf16[1280,128]{1,0:T(8,128)(2,1)} %ed.1, f32[1,2048]{1,0:T(1,128)} %bitcast.6, ...), custom_call_target="tpu_custom_call" | custom-call | tf_op jit(solution)/shard_map/pallas_call | solution.py:395
  102.1 1.9 %copy.15 = bf16[128,2048]{1,0:T(8,128)(2,1)} copy(bf16[128,2048]{1,0:T(8,128)(2,1)} %shard_map.127) | data formatting | bytes 1048576

commit v6 on v5

--- a/solution.py
+++ b/solution.py
@@ -14,39 +14,40 @@
 
 
 ORDER = (
-    ("en", 0), ("en", 1), ("ao", 0, 1, 0), ("ao", 0, 0, 0), ("ao", 0, 0, 1), ("ao", 0, 0, 2), ("ao", 0, 0, 3),
-    ("ao", 0, 1, 1), ("af", 0, 1, 0), ("y", 0, 0), ("af", 0, 0, 0), ("af", 0, 0, 1), ("x", 0, 1), ("y", 0, 1),
-    ("ao", 0, 1, 2), ("ao", 0, 1, 3), ("af", 0, 1, 1), ("y", 0, 2), ("ae", 0, 0), ("x", 0, 3), ("y", 0, 3),
-    ("y", 0, 4), ("ae", 0, 1), ("g1", 0), ("g1", 1), ("x", 0, 5), ("y", 0, 5), ("g2", 1), ("y", 0, 6), ("x", 0, 6),
-    ("g2", 0), ("y", 1, 0), ("x", 1, 1), ("he", 1), ("y", 1, 1), ("he", 0), ("y", 1, 2), ("d", 0, 0, 0),
-    ("d", 0, 0, 1), ("d", 0, 1, 1), ("y", 1, 3), ("d", 0, 1, 0), ("d", 0, 1, 2), ("x", 1, 3), ("y", 1, 4),
-    ("d", 0, 0, 2), ("c", 0, 0, (0, 0)), ("y", 1, 5), ("c", 0, 0, (0, 1)), ("c", 0, 1, (0, 1)), ("d", 0, 0, 3),
-    ("c", 0, 1, (0, 0)), ("x", 1, 5), ("d", 0, 1, 3), ("c", 0, 1, (-1, 0)), ("c", 0, 1, (1, 0)), ("y", 1, 6),
-    ("c", 0, 0, (-1, 0)), ("x", 1, 6), ("d", 0, 0, 4), ("c", 0, 0, (1, 0)), ("d", 0, 0, 5), ("d", 0, 1, 4),
-    ("c", 0, 0, (2, 0)), ("y", 2, 0), ("c", 0, 1, (2, 0)), ("d", 0, 1, 5), ("c", 0, 0, (-1, 1)),
-    ("c", 0, 0, (1, 1)), ("y", 2, 1), ("c", 0, 0, (2, 1)), ("x", 2, 1), ("c", 0, 1, (-1, 1)), ("c", 0, 1, (1, 1)),
-    ("c", 0, 1, (2, 1)), ("y", 2, 2), ("f", 0, 0), ("ao", 1, 0, 0), ("ao", 1, 0, 1), ("ao", 1, 0, 2),
-    ("ao", 1, 0, 3), ("f", 0, 1), ("y", 2, 3), ("x", 2, 3), ("ao", 1, 1, 0), ("af", 1, 0, 0), ("y", 2, 4),
-    ("af", 1, 0, 1), ("ao", 1, 1, 1), ("y", 2, 5), ("x", 2, 5), ("ao", 1, 1, 2), ("af", 1, 1, 0), ("ao", 1, 1, 3),
-    ("y", 2, 6), ("ae", 1, 0), ("gl", 0), ("x", 2, 6), ("y", 3, 0), ("af", 1, 1, 1), ("y", 3, 1), ("x", 3, 1),
-    ("hl", 0), ("d", 1, 0, 0), ("y", 3, 2), ("d", 1, 0, 1), ("y", 3, 3), ("ae", 1, 1), ("gl", 1), ("d", 1, 0, 2),
-    ("x", 3, 3), ("y", 3, 4), ("c", 1, 0, (0, 0)), ("hl", 1), ("d", 1, 1, 0), ("d", 1, 1, 1), ("d", 1, 1, 2),
-    ("c", 1, 0, (0, 1)), ("y", 3, 5), ("x", 3, 5), ("c", 1, 0, (-1, 0)), ("c", 1, 0, (1, 0)), ("d", 1, 1, 3),
-    ("d", 1, 0, 3), ("d", 1, 0, 4), ("c", 1, 1, (0, 0)), ("x", 3, 6), ("y", 3, 6), ("c", 1, 1, (0, 1)),
-    ("c", 1, 1, (-1, 0)), ("c", 1, 1, (1, 0)), ("d", 1, 0, 5), ("d", 1, 1, 5), ("c", 1, 1, (2, 0)), ("d", 1, 1, 4),
-    ("c", 1, 0, (2, 0)), ("c", 1, 0, (-1, 1)), ("c", 1, 0, (1, 1)), ("c", 1, 0, (2, 1)), ("c", 1, 1, (2, 1)),
-    ("c", 1, 1, (-1, 1)), ("c", 1, 1, (1, 1)), ("f", 1, 0), ("f", 1, 1),
+    ("en", 0), ("en", 1), ("ao", 0, 1, 0), ("ao", 0, 0, 0), ("y", 0, 0), ("ao", 0, 1, 1), ("ao", 0, 0, 1),
+    ("x", 0, 1), ("ao", 0, 0, 2), ("af", 0, 1, 0), ("af", 0, 0, 0), ("y", 0, 1), ("y", 0, 2), ("ao", 0, 0, 3),
+    ("ao", 0, 1, 2), ("af", 0, 0, 1), ("y", 0, 3), ("ao", 0, 1, 3), ("x", 0, 3), ("af", 0, 1, 1), ("y", 0, 4),
+    ("y", 0, 5), ("x", 0, 5), ("ae", 0, 0), ("ae", 0, 1), ("g1", 0), ("g1", 1), ("y", 0, 6), ("x", 0, 6),
+    ("g2", 1), ("y", 1, 0), ("g2", 0), ("y", 1, 1), ("x", 1, 1), ("he", 0), ("he", 1), ("y", 1, 2), ("d", 0, 0, 1),
+    ("d", 0, 1, 1), ("y", 1, 3), ("d", 0, 1, 0), ("x", 1, 3), ("d", 0, 0, 0), ("y", 1, 4), ("d", 0, 0, 2),
+    ("y", 1, 5), ("c", 0, 0, (0, 1)), ("d", 0, 1, 2), ("x", 1, 5), ("d", 0, 0, 3), ("d", 0, 1, 3),
+    ("c", 0, 0, (0, 0)), ("y", 1, 6), ("x", 1, 6), ("c", 0, 0, (-1, 0)), ("d", 0, 0, 4), ("d", 0, 0, 5),
+    ("d", 0, 1, 4), ("c", 0, 0, (1, 0)), ("d", 0, 1, 5), ("y", 2, 0), ("c", 0, 0, (-1, 1)), ("c", 0, 0, (2, 0)),
+    ("c", 0, 0, (1, 1)), ("c", 0, 0, (2, 1)), ("c", 0, 1, (0, 0)), ("y", 2, 1), ("c", 0, 1, (2, 0)),
+    ("c", 0, 1, (-1, 0)), ("c", 0, 1, (-1, 1)), ("c", 0, 1, (0, 1)), ("c", 0, 1, (1, 0)), ("c", 0, 1, (1, 1)),
+    ("c", 0, 1, (2, 1)), ("y", 2, 2), ("f", 0, 0), ("ao", 1, 0, 0), ("ao", 1, 0, 1), ("f", 0, 1), ("ao", 1, 1, 0),
+    ("x", 2, 1), ("ao", 1, 0, 2), ("ao", 1, 0, 3), ("y", 2, 3), ("x", 2, 3), ("af", 1, 0, 1), ("y", 2, 4),
+    ("af", 1, 0, 0), ("ao", 1, 1, 1), ("af", 1, 1, 0), ("y", 2, 5), ("x", 2, 5), ("ao", 1, 1, 2), ("ae", 1, 0),
+    ("y", 2, 6), ("x", 2, 6), ("ao", 1, 1, 3), ("gl", 0, 1), ("af", 1, 1, 1), ("gl", 0, 0), ("y", 3, 0),
+    ("x", 3, 1), ("hl", 0), ("y", 3, 1), ("d", 1, 0, 0), ("y", 3, 2), ("d", 1, 0, 1), ("y", 3, 3), ("ae", 1, 1),
+    ("gl", 1, 1), ("gl", 1, 0), ("d", 1, 0, 2), ("x", 3, 3), ("c", 1, 0, (0, 1)), ("y", 3, 4), ("c", 1, 0, (0, 0)),
+    ("y", 3, 5), ("hl", 1), ("d", 1, 1, 1), ("d", 1, 1, 0), ("d", 1, 1, 3), ("x", 3, 5), ("d", 1, 0, 3),
+    ("c", 1, 0, (-1, 0)), ("d", 1, 1, 2), ("y", 3, 6), ("x", 3, 6), ("d", 1, 1, 4), ("d", 1, 0, 5),
+    ("c", 1, 0, (1, 0)), ("d", 1, 1, 5), ("c", 1, 1, (0, 1)), ("d", 1, 0, 4), ("c", 1, 1, (1, 0)),
+    ("c", 1, 1, (-1, 0)), ("c", 1, 1, (1, 1)), ("c", 1, 0, (2, 1)), ("c", 1, 1, (-1, 1)), ("c", 1, 1, (2, 0)),
+    ("c", 1, 1, (2, 1)), ("c", 1, 1, (0, 0)), ("c", 1, 0, (-1, 1)), ("c", 1, 0, (2, 0)), ("c", 1, 0, (1, 1)),
+    ("f", 1, 1), ("f", 1, 0),
 )
 OWN_Y_AT = 4
-OWN_X_AT = 4
+OWN_X_AT = 5
 
 
 def kernel(
     tok, mix, en, eg, ev, ed, ep, mg, ln, lg, lv, ld, lp,
     out,
     gbuf, vbuf, dbuf, xbuf, acc, hbuf, tokv, mixv, mixed, gains,
-    rs1, rr1, rs2, rr2, keep, br, pbuf,
-    loc_sem, w_send, w_recv, p_send, p_recv, ag_send, ag_recv, rs_send, rs1_recv, rs2_recv,
+    rs1, rr1, rs2, rr2, keep, br, pbuf, outv,
+    loc_sem, w_send, w_recv, p_send, p_recv, ag_send, ag_recv, rs_send, rs1_recv, rs2_recv, out_sem,
 ):
     rep = lax.axis_index("rep")
     fs = lax.axis_index("fs")
@@ -274,11 +275,11 @@
         for n in range(5):
             acc[st, :, tile(n)] += dot_rows(st, whole, 1 if st == 0 else -1, tile(n))
 
-    def gemm1_later(h):
+    def gemm1_later(h, part):
         need(2, 19)
         need(2, 20)
         rows = slice(h * 256, h * 256 + 256)
-        for n in range(5):
+        for n in ((0, 1, 2), (3, 4))[part]:
             for st in (0, 1):
                 parts = [dot_rows(st, rows, dy, tile(n), 1) for dy in (0, -1, 1)]
                 acc[st, rows, tile(n)] = parts[0] + parts[1] + parts[2]
@@ -358,7 +359,10 @@
                 mixed[rows, :] = m
                 x_rows(1, h, z, i)[...] = rms(m.astype(F32), gains[3]).astype(BF)
             else:
-                out[rows, :] = (mixed[rows, :].astype(F32) + 0.5 * rms(branch, gains[4])).astype(BF)
+                outv[rows, :] = (mixed[rows, :].astype(F32) + 0.5 * rms(branch, gains[4])).astype(BF)
+        if layer == 1:
+            half = pl.ds(h * 64, 64)
+            pltpu.make_async_copy(outv.at[half], out.at[half], out_sem.at[h]).start()
 
     wait_local(0)
     for sign in (1, -1):
@@ -385,18 +389,38 @@
         await_bytes(units(r, 32), p_send.at[r])
     for layer in (0, 1):
         await_bytes(xbuf.at[0, pl.ds(0, 384), :], ag_send.at[layer])
+    for h in (0, 1):
+        half = pl.ds(h * 64, 64)
+        pltpu.make_async_copy(outv.at[half], out.at[half], out_sem.at[h]).wait()
     await_bytes(rs1, rs_send.at[0])
     await_bytes(rs2, rs_send.at[1])
+
+
+PIECES = 4
+
+
+def settle(source, target, buf, in_sem, out_sem):
+    rows = 128 // PIECES
+    parts = [pl.ds(i * rows, rows) for i in range(PIECES)]
+    arrive = [pltpu.make_async_copy(source.at[p], buf.at[p], in_sem.at[i]) for i, p in enumerate(parts)]
+    leave = [pltpu.make_async_copy(buf.at[p], target.at[p], out_sem.at[i]) for i, p in enumerate(parts)]
+    for copy in arrive:
+        copy.start()
+    for i in range(PIECES):
+        arrive[i].wait()
+        leave[i].start()
+    for copy in leave:
+        copy.wait()
 
 
 def on_device(tokens, mixer_output, en, eg, ev, ed, ep, mg, ln, lg, lv, ld, lp):
     gains = [g.reshape(1, 2048) for g in (en, ep, mg, ln, lp)]
     en, ep, mg, ln, lp = gains
-    return pl.pallas_call(
+    result = pl.pallas_call(
         kernel,
         out_shape=jax.ShapeDtypeStruct((128, 2048), BF),
         in_specs=[pl.BlockSpec(memory_space=pl.ANY)] * 13,
-        out_specs=pl.BlockSpec(memory_space=pltpu.VMEM),
+        out_specs=pl.BlockSpec(memory_space=pl.ANY),
         scratch_shapes=[
             pltpu.VMEM((2, 2048, 1280), BF),
             pltpu.VMEM((2, 2048, 1280), BF),
@@ -415,6 +439,7 @@
             pltpu.VMEM((2, 8, 2, 32, 256), F32),
             pltpu.VMEM((128, 2048), F32),
             pltpu.VMEM((2, 256, 256), F32),
+            pltpu.VMEM((128, 2048), BF),
             pltpu.SemaphoreType.DMA((7,)),
             pltpu.SemaphoreType.DMA((4,)),
             pltpu.SemaphoreType.DMA((4, 11)),
@@ -425,11 +450,21 @@
             pltpu.SemaphoreType.DMA((2,)),
             pltpu.SemaphoreType.DMA((2, 8)),
             pltpu.SemaphoreType.DMA((2,)),
+            pltpu.SemaphoreType.DMA((2,)),
         ],
         compiler_params=pltpu.CompilerParams(
             collective_id=0, has_side_effects=True, vmem_limit_bytes=67_000_000
         ),
     )(tokens, mixer_output, en, eg, ev, ed, ep, mg, ln, lg, lv, ld, lp)
+    return pl.pallas_call(
+        settle,
+        out_shape=jax.ShapeDtypeStruct((128, 2048), BF),
+        in_specs=[pl.BlockSpec(memory_space=pl.ANY)],
+        out_specs=pl.BlockSpec(memory_space=pl.ANY),
+        scratch_shapes=[
+            pltpu.VMEM((128, 2048), BF), pltpu.SemaphoreType.DMA((PIECES,)), pltpu.SemaphoreType.DMA((PIECES,))
+        ],
+    )(result)
 
 
 def solution(mesh):

time: 105 us -> 104 us (level)
  local copies, waits for them, and re-layouts: 1.88 us -> 0 us
    unnamed x1 -> x0, local copies, waits for them, and re-layouts: 1.88 us -> none
    pallas_call x0 -> x1, Pallas kernels: none -> 1.82 us  [on_device(): pl.pallas_call(settle, out_shape=jax.ShapeDtypeStruct((128, 2048), BF), i...]
where the time goes in v6:
time: 104 us; the launch traced here: 103 us
  Pallas kernels  103 us (99%)
    pallas_call x1, Pallas kernels, on_device(): pl.pallas_call(kernel, out_shape=jax.ShapeDtypeStruct((128, 2048), BF), i...  101 us

profile of v6, /device:TPU:1, one launch (start us, length us, event | category | flops | bytes accessed | tf_op | source)
XLA Modules:
  0.0 103.4 jit_solution(2598072472201372433)
XLA Ops:
  0.0 101.4 %shard_map.127.source = bf16[128,2048]{1,0:T(8,128)(2,1)} custom-call(bf16[128,2048]{1,0:T(8,128)(2,1)} %tok.1, bf16[128,2048]{1,0:T(8,128)(2,1)} %mix.1, f32[1,2048]{1,0:T(1,128)} %bitcast.5, bf16[128,1280]{1,0:T(8,128)(2,1)} %eg.1, bf16[128,1280]{1,0:T(8,128)(2,1)} %ev.1, bf16[1280,128]{1,0:T(8,128)(2,1)} %ed.1, f32[1,2048]{1,0:T(1,128)} %bitcast.6, ...), custom_call_target="tpu_custom_call" | custom-call | tf_op jit(solution)/shard_map/pallas_call | solution.py:419
  101.4 1.8 %shard_map.128 = bf16[128,2048]{1,0:T(8,128)(2,1)} custom-call(bf16[128,2048]{1,0:T(8,128)(2,1)} %shard_map.127.source), custom_call_target="tpu_custom_call" | custom-call | tf_op jit(solution)/shard_map/pallas_call | solution.py:459

commit v7 on v6

--- a/solution.py
+++ b/solution.py
@@ -46,8 +46,8 @@
     tok, mix, en, eg, ev, ed, ep, mg, ln, lg, lv, ld, lp,
     out,
     gbuf, vbuf, dbuf, xbuf, acc, hbuf, tokv, mixv, mixed, gains,
-    rs1, rr1, rs2, rr2, keep, br, pbuf, outv,
-    loc_sem, w_send, w_recv, p_send, p_recv, ag_send, ag_recv, rs_send, rs1_recv, rs2_recv, out_sem,
+    rs1, rr1, rs2, rr2, keep, br, pbuf,
+    loc_sem, w_send, w_recv, p_send, p_recv, ag_send, ag_recv, rs_send, rs1_recv, rs2_recv,
 ):
     rep = lax.axis_index("rep")
     fs = lax.axis_index("fs")
@@ -359,10 +359,7 @@
                 mixed[rows, :] = m
                 x_rows(1, h, z, i)[...] = rms(m.astype(F32), gains[3]).astype(BF)
             else:
-                outv[rows, :] = (mixed[rows, :].astype(F32) + 0.5 * rms(branch, gains[4])).astype(BF)
-        if layer == 1:
-            half = pl.ds(h * 64, 64)
-            pltpu.make_async_copy(outv.at[half], out.at[half], out_sem.at[h]).start()
+                out[rows, :] = (mixed[rows, :].astype(F32) + 0.5 * rms(branch, gains[4])).astype(BF)
 
     wait_local(0)
     for sign in (1, -1):
@@ -389,38 +386,18 @@
         await_bytes(units(r, 32), p_send.at[r])
     for layer in (0, 1):
         await_bytes(xbuf.at[0, pl.ds(0, 384), :], ag_send.at[layer])
-    for h in (0, 1):
-        half = pl.ds(h * 64, 64)
-        pltpu.make_async_copy(outv.at[half], out.at[half], out_sem.at[h]).wait()
     await_bytes(rs1, rs_send.at[0])
     await_bytes(rs2, rs_send.at[1])
-
-
-PIECES = 4
-
-
-def settle(source, target, buf, in_sem, out_sem):
-    rows = 128 // PIECES
-    parts = [pl.ds(i * rows, rows) for i in range(PIECES)]
-    arrive = [pltpu.make_async_copy(source.at[p], buf.at[p], in_sem.at[i]) for i, p in enumerate(parts)]
-    leave = [pltpu.make_async_copy(buf.at[p], target.at[p], out_sem.at[i]) for i, p in enumerate(parts)]
-    for copy in arrive:
-        copy.start()
-    for i in range(PIECES):
-        arrive[i].wait()
-        leave[i].start()
-    for copy in leave:
-        copy.wait()
 
 
 def on_device(tokens, mixer_output, en, eg, ev, ed, ep, mg, ln, lg, lv, ld, lp):
     gains = [g.reshape(1, 2048) for g in (en, ep, mg, ln, lp)]
     en, ep, mg, ln, lp = gains
-    result = pl.pallas_call(
+    return pl.pallas_call(
         kernel,
-        out_shape=jax.ShapeDtypeStruct((128, 2048), BF),
+        out_shape=pltpu.VMEM((128, 2048), BF),
         in_specs=[pl.BlockSpec(memory_space=pl.ANY)] * 13,
-        out_specs=pl.BlockSpec(memory_space=pl.ANY),
+        out_specs=pl.BlockSpec(memory_space=pltpu.VMEM),
         scratch_shapes=[
             pltpu.VMEM((2, 2048, 1280), BF),
             pltpu.VMEM((2, 2048, 1280), BF),
@@ -439,7 +416,6 @@
             pltpu.VMEM((2, 8, 2, 32, 256), F32),
             pltpu.VMEM((128, 2048), F32),
             pltpu.VMEM((2, 256, 256), F32),
-            pltpu.VMEM((128, 2048), BF),
             pltpu.SemaphoreType.DMA((7,)),
             pltpu.SemaphoreType.DMA((4,)),
             pltpu.SemaphoreType.DMA((4, 11)),
@@ -450,21 +426,11 @@
             pltpu.SemaphoreType.DMA((2,)),
             pltpu.SemaphoreType.DMA((2, 8)),
             pltpu.SemaphoreType.DMA((2,)),
-            pltpu.SemaphoreType.DMA((2,)),
         ],
         compiler_params=pltpu.CompilerParams(
-            collective_id=0, has_side_effects=True, vmem_limit_bytes=67_000_000
+            collective_id=0, has_side_effects=True, vmem_limit_bytes=60_000_000
         ),
     )(tokens, mixer_output, en, eg, ev, ed, ep, mg, ln, lg, lv, ld, lp)
-    return pl.pallas_call(
-        settle,
-        out_shape=jax.ShapeDtypeStruct((128, 2048), BF),
-        in_specs=[pl.BlockSpec(memory_space=pl.ANY)],
-        out_specs=pl.BlockSpec(memory_space=pl.ANY),
-        scratch_shapes=[
-            pltpu.VMEM((128, 2048), BF), pltpu.SemaphoreType.DMA((PIECES,)), pltpu.SemaphoreType.DMA((PIECES,))
-        ],
-    )(result)
 
 
 def solution(mesh):

time: 104 us -> 102 us (0.981)
  Pallas kernels: 103 us -> 101 us
    pallas_call x2 -> x1, Pallas kernels: 103 us -> 101 us  [on_device(): pl.pallas_call(kernel, out_shape=pltpu.VMEM((128, 2048), BF), in_specs=[p...]
where the time goes in v7:
time: 102 us
  Pallas kernels  101 us (99%)
    pallas_call x1, Pallas kernels, on_device(): pl.pallas_call(kernel, out_shape=pltpu.VMEM((128, 2048), BF), in_specs=[p...  101 us

profile of v7, /device:TPU:1, one launch (start us, length us, event | category | flops | bytes accessed | tf_op | source)
XLA Modules:
  0.0 101.5 jit_solution(17518846867811946822)
XLA Ops:
  0.0 100.7 %shard_map.127 = bf16[128,2048]{1,0:T(8,128)(2,1)S(1)} custom-call(bf16[128,2048]{1,0:T(8,128)(2,1)} %tok.1, bf16[128,2048]{1,0:T(8,128)(2,1)} %mix.1, f32[1,2048]{1,0:T(1,128)} %bitcast.5, bf16[128,1280]{1,0:T(8,128)(2,1)} %eg.1, bf16[128,1280]{1,0:T(8,128)(2,1)} %ev.1, bf16[1280,128]{1,0:T(8,128)(2,1)} %ed.1, f32[1,2048]{1,0:T(1,128)} %bitcast.6, ...), custom_call_target="tpu_custom_call" | custom-call | tf_op jit(solution)/shard_map/pallas_call | solution.py:396
  100.7 0.8 copy.15

commit v8 on v7

--- a/solution.py
+++ b/solution.py
@@ -212,6 +212,10 @@
     for i, pairs in enumerate((weights[0], [(tok, tokv)], norms, weights[1], weights[2], weights[3], [(mix, mixv)])):
         for src, dst in pairs:
             pltpu.make_async_copy(src, dst, loc_sem.at[i]).start()
+        if i == 0:
+            barrier = pltpu.get_barrier_semaphore()
+            for other in everyone:
+                pl.semaphore_signal(barrier, inc=1, device_id=other, device_id_type=MESH)
 
     def wait_local(r):
         await_bytes(units(r, 4), loc_sem.at[(0, 3, 4, 5)[r]])
@@ -219,9 +223,6 @@
             for s in (0, 1):
                 have.add((r, (0, 0, st, s)))
 
-    barrier = pltpu.get_barrier_semaphore()
-    for other in everyone:
-        pl.semaphore_signal(barrier, inc=1, device_id=other, device_id_type=MESH)
     pl.semaphore_wait(barrier, len(everyone))
 
     def x_rows(layer, h, zz, u, n=16):

time: 102 us -> 102 us (level)
  no operation moved by 1% of the time
where the time goes in v8:
time: 102 us
  Pallas kernels  101 us (99%)
    pallas_call x1, Pallas kernels, on_device(): pl.pallas_call(kernel, out_shape=pltpu.VMEM((128, 2048), BF), in_specs=[p...  101 us

profile of v8, /device:TPU:1, one launch (start us, length us, event | category | flops | bytes accessed | tf_op | source)
XLA Modules:
  0.0 101.5 jit_solution(13370202427377191054)
XLA Ops:
  0.0 100.7 %shard_map.127 = bf16[128,2048]{1,0:T(8,128)(2,1)S(1)} custom-call(bf16[128,2048]{1,0:T(8,128)(2,1)} %tok.1, bf16[128,2048]{1,0:T(8,128)(2,1)} %mix.1, f32[1,2048]{1,0:T(1,128)} %bitcast.5, bf16[128,1280]{1,0:T(8,128)(2,1)} %eg.1, bf16[128,1280]{1,0:T(8,128)(2,1)} %ev.1, bf16[1280,128]{1,0:T(8,128)(2,1)} %ed.1, f32[1,2048]{1,0:T(1,128)} %bitcast.6, ...), custom_call_target="tpu_custom_call" | custom-call | tf_op jit(solution)/shard_map/pallas_call | solution.py:397
  100.7 0.8 copy.15

commit v9 on v7

--- a/solution.py
+++ b/solution.py
@@ -39,7 +39,7 @@
     ("f", 1, 1), ("f", 1, 0),
 )
 OWN_Y_AT = 4
-OWN_X_AT = 5
+OWN_X_AT = 4
 
 
 def kernel(

time: 102 us -> 102 us (level)
  no operation moved by 1% of the time
where the time goes in v9:
time: 102 us
  Pallas kernels  101 us (99%)
    pallas_call x1, Pallas kernels, on_device(): pl.pallas_call(kernel, out_shape=pltpu.VMEM((128, 2048), BF), in_specs=[p...  101 us

profile of v9, /device:TPU:1, one launch (start us, length us, event | category | flops | bytes accessed | tf_op | source)
XLA Modules:
  0.0 101.5 jit_solution(338732695871666940)
XLA Ops:
  0.0 100.7 %shard_map.127 = bf16[128,2048]{1,0:T(8,128)(2,1)S(1)} custom-call(bf16[128,2048]{1,0:T(8,128)(2,1)} %tok.1, bf16[128,2048]{1,0:T(8,128)(2,1)} %mix.1, f32[1,2048]{1,0:T(1,128)} %bitcast.5, bf16[128,1280]{1,0:T(8,128)(2,1)} %eg.1, bf16[128,1280]{1,0:T(8,128)(2,1)} %ev.1, bf16[1280,128]{1,0:T(8,128)(2,1)} %ed.1, f32[1,2048]{1,0:T(1,128)} %bitcast.6, ...), custom_call_target="tpu_custom_call" | custom-call | tf_op jit(solution)/shard_map/pallas_call | solution.py:396
  100.7 0.8 copy.15
